TPU v7x, 32 devices: a whole 2x2x4 slice. The times are simulated.
32 devices in a mesh: grp: 1, sp: 16 (over z, y, core), tp: 2 (over x).
Axes of the slice: x: 2, y: 2, z: 4, core: 2. Of those that a mesh axis runs over, the one named last changes fastest.
Arguments:
- residual_in: bfloat16 [2048, 2048], P(('grp', 'sp'), 'tp'), may hold values from -16 to 16
- query_pre: bfloat16 [2048, 512], P(('grp', 'sp'), 'tp'), may hold values from -6 to 6
- forget_pre: bfloat16 [2048, 512], P(('grp', 'sp'), 'tp'), may hold values from -9 to 9
- value_pre: bfloat16 [2048, 512], P(('grp', 'sp'), 'tp'), may hold values from -6 to 6
- gate_pre: bfloat16 [2048, 512], P(('grp', 'sp'), 'tp'), may hold values from -6 to 6
- floor_gap: float32 [512], P('tp'), may hold values from 0 to 1, as said below
- head_gain: float32 [64], replicated, may hold values from 0.1 to 1.9
- out_weight: bfloat16 [512, 2048], P(None, 'tp'), may hold values from -0.25 to 0.25
- norm_gain: float32 [2048], P('tp'), may hold values from 0.1 to 1.9
- value_weight: bfloat16 [2048, 5632], P('sp', 'tp'), may hold values from -0.125 to 0.125
- gate_weight: bfloat16 [2048, 5632], P('sp', 'tp'), may hold values from -0.125 to 0.125
- value_taps: float32 [3, 5632], P(None, 'tp'), may hold values from -3 to 3
- gate_taps: float32 [3, 5632], P(None, 'tp'), may hold values from -3 to 3
- down_weight: bfloat16 [5632, 2048], P('tp', 'sp'), may hold values from -0.078125 to 0.078125
Outputs:
- mixed: bfloat16 [2048, 2048], P(('grp', 'sp'), 'tp')
Inputs may be any that keep to these rules, and one draw needn't show every extreme that they name: `floor_gap`: each channel's value lies strictly between 0 and 1.
All inputs are finite; a program needn't handle non-finite values.
Results may differ from a plain program's by a relative error of at most 0.0085.
Values may be sent and summed in bfloat16 or wider, within the bound.
A program may use at most 128 MiB of HBM per device.

v0:
```python
import jax
import jax.numpy as jnp
from jax import lax
from jax.sharding import PartitionSpec as P

DK = 64
SUB = 16
epsilon = 1e-06
highest = lax.Precision.HIGHEST
f32 = jnp.float32
bf16 = jnp.bfloat16


def local_recurrence(query_pre, forget_pre, value_pre, floor_gap):
    rows, width = query_pre.shape
    heads = width // DK
    subs = rows // SUB
    keys = floor_gap * jax.nn.sigmoid(-forget_pre.astype(f32))
    log_decay = jnp.log1p(-keys)
    query = jax.nn.silu(query_pre.astype(f32))
    values = value_pre.astype(f32)
    position = lax.iota(jnp.int32, rows)
    lower = (position[:, None] >= position[None, :]).astype(f32)
    running = jnp.dot(lower, log_decay, precision=highest)
    middle = running.reshape(subs, SUB, width)[:, SUB // 2 - 1, :]
    query_part = query * jnp.exp(running - jnp.repeat(middle, SUB, axis=0))
    reach = (lax.iota(jnp.int32, subs) + 1) * SUB
    seen = position[None, :, None] < reach[:, None, None]
    key_part = keys[None] * jnp.exp(
        jnp.where(seen, middle[:, None, :] - running[None], -jnp.inf)
    )
    scores = jnp.einsum(
        "ithk,ishk->hits",
        query_part.reshape(subs, SUB, heads, DK),
        key_part.reshape(subs, rows, heads, DK),
        precision=highest,
    ).reshape(heads, rows, rows)
    scores = jnp.where(position[None, :, None] >= position[None, None, :], scores, 0.0)
    value_heads = values.reshape(rows, heads, DK)
    inner = jnp.einsum("hts,shv->htv", scores, value_heads, precision=highest)
    ending = running[-1]
    state = jnp.einsum(
        "shv,shk->vhk",
        value_heads,
        (keys * jnp.exp(ending - running)).reshape(rows, heads, DK),
        precision=highest,
    ).reshape(DK, width)
    from_start = (query * jnp.exp(running)).reshape(rows, heads, DK)
    return inner, state, jnp.exp(ending), from_start


def causal_taps(before, current, taps):
    padded = jnp.concatenate([before, current], axis=1).astype(f32)
    rows = current.shape[1]
    return (
        taps[0] * padded[:, 0:rows]
        + taps[1] * padded[:, 1 : rows + 1]
        + taps[2] * padded[:, 2 : rows + 2]
    )


def on_device(
    residual_in,
    query_pre,
    forget_pre,
    value_pre,
    gate_pre,
    floor_gap,
    head_gain,
    out_weight,
    norm_gain,
    value_weight,
    gate_weight,
    value_taps,
    gate_taps,
    down_weight,
):
    sp = lax.axis_size("sp")
    tp = lax.axis_size("tp")
    inner_size = 4 if sp % 4 == 0 else 1
    outer = sp // inner_size
    me = lax.axis_index("sp")
    my_outer = me // inner_size
    my_inner = me % inner_size
    outer_groups = [[o * inner_size + i for o in range(outer)] for i in range(inner_size)]
    inner_groups = [[o * inner_size + i for i in range(inner_size)] for o in range(outer)]
    rows, my_width = residual_in.shape
    width = my_width * tp
    depth, half = value_weight.shape
    chunk = half // outer

    wide_groups = [
        [s * tp + t for s in group for t in range(tp)] for group in outer_groups
    ]

    def exchange(array):
        return lax.all_to_all(
            array, "sp", 0, 0, axis_index_groups=outer_groups, tiled=True
        )

    def gather_inner(array):
        return lax.all_gather(array, "sp", axis_index_groups=inner_groups)

    def gather_wide(array):
        gathered = lax.all_gather(array, ("sp", "tp"), axis_index_groups=wide_groups)
        gathered = gathered.reshape(outer, tp, *array.shape)
        return [gathered[:, t].reshape(-1, array.shape[1]) for t in range(tp)]

    def reorder(pieces):
        span = pieces[0].shape[-1]
        blocks = []
        for i in range(inner_size):
            for o in range(outer):
                start = (o * inner_size + i) * depth
                low = start % span
                blocks.append(pieces[start // span][..., low : low + depth])
        return lax.optimization_barrier(jnp.concatenate(blocks, axis=-1))

    up_parts = jnp.stack(
        [
            jnp.concatenate(
                [
                    value_weight[:, o * chunk : (o + 1) * chunk],
                    gate_weight[:, o * chunk : (o + 1) * chunk],
                ],
                axis=1,
            )
            for o in range(outer)
        ]
    )
    up_chunk = gather_inner(exchange(up_parts)).reshape(width, 2 * chunk)
    down_parts = down_weight.reshape(outer, chunk, depth)
    down_mine = gather_inner(exchange(down_parts))
    down_chunk = down_mine.transpose(2, 1, 0, 3).reshape(chunk, width)

    out_full = reorder(list(lax.all_gather(out_weight, "tp")))
    gain_full = reorder(list(lax.all_gather(norm_gain, "tp")))
    residual_group = reorder(gather_wide(residual_in))

    inner, state, total_decay, from_start = local_recurrence(
        query_pre, forget_pre, value_pre, floor_gap
    )
    heads = inner.shape[0]
    first = total_decay.astype(bf16)
    rest = total_decay - first.astype(f32)
    second = rest.astype(bf16)
    third = (rest - second.astype(f32)).astype(bf16)
    spare = jnp.zeros((13, heads * DK), bf16)
    packed = jnp.concatenate(
        [state.astype(bf16), first[None], second[None], third[None], spare], axis=0
    )
    everyone = lax.all_gather(packed, "sp").astype(f32)
    decays = everyone[:, DK] + everyone[:, DK + 1] + everyone[:, DK + 2]
    entering = jnp.zeros_like(state)
    for j in range(sp - 1):
        advanced = entering * decays[j] + everyone[j, :DK]
        entering = jnp.where(j < me, advanced, entering)
    carried = jnp.einsum(
        "thk,vhk->htv", from_start, entering.reshape(DK, heads, DK), precision=highest
    )
    recurrent = (inner + carried).transpose(1, 0, 2)
    scaled = (
        recurrent
        * lax.rsqrt(jnp.mean(recurrent * recurrent, axis=-1, keepdims=True) + epsilon)
        * head_gain
    )
    gating = jax.nn.silu(gate_pre.astype(f32)).reshape(recurrent.shape)
    head_out = (scaled * gating).reshape(rows, heads * DK).astype(bf16)

    head_out, out_full = lax.optimization_barrier((head_out, out_full))
    head_group = jnp.concatenate(gather_wide(head_out), axis=1)
    stream = residual_group.astype(f32) + jnp.dot(
        head_group, out_full, preferred_element_type=f32
    )
    squares = jnp.mean(stream * stream, axis=1, keepdims=True)
    normed = (stream * lax.rsqrt(squares + epsilon) * gain_full).astype(bf16)
    up = jnp.dot(normed, up_chunk, preferred_element_type=f32).astype(bf16)
    up = up.reshape(outer, rows, 2 * chunk)
    tails = up[:, rows - 2 :]
    pairs = [
        (o * inner_size + i, o * inner_size + (i + 1) % inner_size)
        for o in range(outer)
        for i in range(inner_size)
    ]
    arrived = lax.ppermute(tails, "sp", pairs) if inner_size > 1 else tails
    wrapped = jnp.concatenate([jnp.zeros_like(arrived[:1]), arrived[:-1]], axis=0)
    before = jnp.where(my_inner == 0, wrapped, arrived)

    taps = jnp.concatenate(
        [
            lax.dynamic_slice_in_dim(value_taps, my_outer * chunk, chunk, axis=1),
            lax.dynamic_slice_in_dim(gate_taps, my_outer * chunk, chunk, axis=1),
        ],
        axis=1,
    )
    conv = causal_taps(before, up, taps)
    hidden = (jax.nn.silu(conv[:, :, chunk:]) * conv[:, :, :chunk]).astype(bf16)
    terms = jnp.dot(
        hidden.reshape(outer * rows, chunk), down_chunk, preferred_element_type=f32
    ).astype(bf16)
    summed = lax.psum_scatter(
        terms, "sp", scatter_dimension=0, tiled=True, axis_index_groups=outer_groups
    )
    summed = lax.psum_scatter(summed, "tp", scatter_dimension=1, tiled=True)
    my_heads = lax.dynamic_slice_in_dim(head_group, my_outer * rows, rows, axis=0)
    own = residual_in.astype(f32) + jnp.dot(
        my_heads, out_weight, preferred_element_type=f32
    )
    return (own + summed.astype(f32)).astype(bf16)


def solution(mesh):
    rows = P(("grp", "sp"), "tp")
    return jax.shard_map(
        on_device,
        mesh=mesh,
        in_specs=(
            rows,
            rows,
            rows,
            rows,
            rows,
            P("tp"),
            P(),
            P(None, "tp"),
            P("tp"),
            P("sp", "tp"),
            P("sp", "tp"),
            P(None, "tp"),
            P(None, "tp"),
            P("tp", "sp"),
        ),
        out_specs=rows,
        check_vma=False,
    )
```

profile of v0, /device:TPU:0, one launch (start us, length us, event | category | flops | bytes accessed | tf_op | source)
XLA Modules:
  0.0 262.0 jit_solution(9370654994997921655)
XLA Ops:
  6.5 0.7 all-gather.12.cloned.1.call-update
  7.3 0.7 all-gather.14.cloned.1.call-update
  8.1 1.4 fusion.41
  9.5 0.2 fusion.42
  9.7 0.2 maximum_bitcast_fusion
  9.9 0.2 maximum_bitcast_fusion.2
  10.1 0.2 pad_maximum_fusion
  10.4 40.4 %all_to_all.10 = bf16[4,128,1408]{2,1,0:T(8,128)(2,1)} all-to-all(bf16[4,128,1408]{2,1,0:T(8,128)(2,1)S(1)} %pad_maximum_fusion), channel_id=1, replica_groups={{0,8,16,24},{2,10,18,26},{4,12,20,28},{6,14,22,30},{1,9,17,25},{3,11,19..., dimensions={0} | all-to-all | bytes 2883584 | tf_op jit(solution)/shard_map/all_to_all | solution.py:97
  50.8 3.6 %all-to-all-start.1 = ((bf16[4,704,128]{2,1,0:T(8,128)(2,1)}), bf16[4,704,128]{2,1,0:T(8,128)(2,1)S(1)}, u32[]{:S(2)}, u32[]{:S(2)}) async-start(bf16[4,704,128]{2,1,0:T(8,128)(2,1)} %bitcast.45), calls=%async_computation.1 | async-start | bytes 1441792 | tf_op jit(solution)/shard_map/all_to_all | solution.py:97
  54.6 0.3 fusion.30
  54.9 0.8 copy.57
  55.7 0.1 exponential_multiply_fusion.1
  56.1 0.2 convolution_convert_fusion.2
  56.4 0.2 concatenate.36
  56.6 35.8 %all-gather = bf16[1280,256]{1,0:T(8,128)(2,1)S(1)} all-gather(bf16[80,256]{1,0:T(8,128)(2,1)S(1)} %concatenate.36), channel_id=2, replica_groups=mesh['grp'=1,'sp'=16,'tp'=2] {'sp'}, dimensions={0}, use_global_device_ids=true | all-gather | bytes 696320 | tf_op jit(solution)/shard_map/all_gather | solution.py:152
  92.4 0.1 convert
  92.6 0.2 reshape.266
  92.9 4.4 %all-gather.4 = f32[2048]{0:T(1024)S(1)} all-gather(f32[1024]{0:T(1024)S(1)} %copy-done.9), channel_id=6, replica_groups=mesh['grp'=1,'sp'=16,'tp'=2] {'tp'}, dimensions={0}, use_global_device_ids=true | all-gather | bytes 12288 | tf_op jit(solution)/shard_map/all_gather | solution.py:137
  97.6 0.9 convert_multiply_fusion
  98.5 2.1 fusion.8
  100.7 0.4 fusion.46
  102.5 0.1 squeeze.54
  102.9 0.1 squeeze.57
  103.0 0.1 squeeze.58
  103.1 0.1 squeeze.59
  103.5 0.1 squeeze.62
  103.6 0.1 squeeze.63
  103.7 0.1 squeeze.64
  104.4 0.4 add_select_fusion
  104.9 0.3 multiply_reduce_fusion.1
  105.3 0.9 copy-done.2
  106.2 0.9 slice_dynamic-update-slice_fusion.31
  107.2 0.9 slice_dynamic-update-slice_fusion.30
  108.1 0.9 slice_dynamic-update-slice_fusion.29
  109.1 0.9 slice_dynamic-update-slice_fusion.28
  110.0 0.9 slice_dynamic-update-slice_fusion.27
  111.0 0.9 slice_dynamic-update-slice_fusion.26
  111.9 1.0 slice_dynamic-update-slice_fusion.25
  112.9 1.0 slice_dynamic-update-slice_fusion.24
  113.9 1.0 slice_dynamic-update-slice_fusion.23
  114.9 0.9 slice_dynamic-update-slice_fusion.22
  115.8 1.0 slice_dynamic-update-slice_fusion.21
  116.8 1.0 slice_dynamic-update-slice_fusion.20
  117.8 0.9 slice_dynamic-update-slice_fusion.19
  118.7 0.9 slice_dynamic-update-slice_fusion.18
  119.7 0.9 slice_dynamic-update-slice_fusion.17
  120.6 0.9 slice_dynamic-update-slice_fusion.16
  121.7 32.7 %all-gather.2 = bf16[1024,256]{1,0:T(8,128)(2,1)S(1)} all-gather(bf16[128,256]{1,0:T(8,128)(2,1)S(1)} %copy.65), channel_id=4, replica_groups={{0,1,8,9,16,17,24,25},{2,3,10,11,18,19,26,27},{4,5,12,13,20,21,28,29},{..., dimensions={0}, use_global_device_ids=true | all-gather | bytes 589824 | tf_op jit(solution)/shard_map/all_gather | solution.py:105
  154.4 1.7 fusion.40
  157.1 3.4 %multiply_reduce_fusion = (f32[512]{0:T(512)S(1)}, f32[512,2048]{1,0:T(8,128)}) fusion(bf16[512,2048]{1,0:T(8,128)(2,1)S(1)} %slice_dynamic-update-slice_fusion.16, bf16[512,256]{1,0:T(8,128)(2,1)S(1)} %bitcast.147, bf16[512,256]{1,0:T(8,128)(2,1)S(1)} %bitcast.145, bf16[512,2048]{1,0:T(8,128)(2,1)S(1)} %slice_dynamic-update-slice_fusion), kind=kOutput, calls=%fused_computation.1 | convolution fusion | flops 1078984192 | bytes 8914944 | tf_op jit(solution)/shard_map/dot_general | solution.py:172
  160.5 7.4 %convolution_convert_fusion.1 = bf16[512,1408]{1,0:T(8,128)(2,1)S(1)} fusion(bf16[2048,1408]{1,0:T(8,128)(2,1)} %bitcast.166, f32[512,2048]{1,0:T(8,128)} %get-tuple-element.66, f32[2048]{0:T(1024)S(1)} %constant_dynamic-update-slice_fusion.1, f32[512]{0:T(512)S(1)} %add_rsqrt_fusion), kind=kOutput, calls=%fused_computation.4 | convolution fusion | flops 2956656640 | bytes 11413504 | tf_op jit(solution)/shard_map/dot_general | solution.py:177
  167.8 1.1 copy-done.3
  169.0 0.8 constant_dynamic-slice_fusion
  170.0 8.5 %all-gather.18.cloned.1.call-done = bf16[16,704,128]{2,1,0:T(8,128)(2,1)} async-done(((bf16[4,704,128]{2,1,0:T(8,128)(2,1)}), bf16[16,704,128]{2,1,0:T(8,128)(2,1)}) %all-gather.18.cloned.1.call-update) | async-done | bytes 2883600 | tf_op jit(solution)/shard_map/all_gather | solution.py:102
  178.5 4.0 %copy.68 = bf16[704,4,4,128]{3,2,1,0:T(4,128)(2,1)S(1)} copy(bf16[704,4,4,128]{3,0,1,2:T(8,128)(2,1)} %bitcast.144) | data formatting | bytes 5767168 | tf_op jit(solution)/shard_map/transpose | solution.py:134
  182.5 3.4 %reshape.278 = bf16[704,2048]{1,0:T(8,128)(2,1)} reshape(bf16[704,4,4,128]{3,2,1,0:T(4,128)(2,1)S(1)} %copy.68) | data formatting | bytes 5767168 | tf_op jit(solution)/shard_map/reshape | solution.py:134
  185.9 1.7 maximum_convert_fusion
  187.6 0.8 fusion
  188.5 0.5 fusion.4
  189.0 1.3 copy-done.1
  190.3 3.1 %convolution_convert_fusion = bf16[512,2048]{1,0:T(8,128)(2,1)} fusion(bf16[512,704]{1,0:T(8,128)(2,1)S(1)} %bitcast.153, bf16[704,2048]{1,0:T(8,128)(2,1)S(1)} %copy-done.1), kind=kOutput, calls=%fused_computation.3 | convolution fusion | flops 1477443584 | bytes 5701632 | tf_op jit(solution)/shard_map/dot_general | solution.py:198
  193.5 43.7 %reduce-scatter.3.cloned.1.call-done = bf16[128,2048]{1,0:T(8,128)(2,1)} async-done(((bf16[512,2048]{1,0:T(8,128)(2,1)}), bf16[128,2048]{1,0:T(8,128)(2,1)}) %reduce-scatter.3.cloned.1.call-update) | async-done | bytes 524304 | tf_op jit(solution)/shard_map/reduce_scatter | solution.py:201
  237.3 15.9 %reduce-scatter.5.cloned.1.call-done = bf16[128,1024]{1,0:T(8,128)(2,1)} async-done(((bf16[128,2048]{1,0:T(8,128)(2,1)}), bf16[128,1024]{1,0:T(8,128)(2,1)}) %reduce-scatter.5.cloned.1.call-update) | async-done | bytes 262160 | tf_op jit(solution)/shard_map/reduce_scatter | solution.py:204
  253.2 2.0 fusion.6
  (122 shorter events, 4.9 us)
Async XLA Ops:
  6.5 2.9 %copy-start.5 = (bf16[128,2816]{1,0:T(8,128)(2,1)S(1)}, bf16[128,2816]{1,0:T(8,128)(2,1)}, u32[]{:S(2)}) copy-start(bf16[128,2816]{1,0:T(8,128)(2,1)} %param.24) | copy-start | bytes 2162692
  6.5 99.7 %all-gather.12.cloned.1.call-start = ((), (), s32[]{:S(2)}) async-start(), calls=%async_computation.6 | async-start | bytes 3145728 | tf_op jit(solution)/shard_map/all_gather | solution.py:136
  7.3 147.2 %all-gather.14.cloned.1.call-start = ((), (), s32[]{:S(2)}) async-start(), calls=%async_computation.7 | async-start | bytes 2359296 | tf_op jit(solution)/shard_map/all_gather | solution.py:105
  8.0 152.5 %all-gather.16.cloned.1.call-start = ((), (), s32[]{:S(2)}) async-start(), calls=%async_computation.8 | async-start | bytes 7208960 | tf_op jit(solution)/shard_map/all_gather | solution.py:102
  50.8 3.8 %copy-start.6 = (bf16[128,256]{1,0:T(8,128)(2,1)S(1)}, bf16[128,256]{1,0:T(8,128)(2,1)}, u32[]{:S(2)}) copy-start(bf16[128,256]{1,0:T(8,128)(2,1)} %param.16) | copy-start | bytes 196612
  50.8 3.8 %copy-start.10 = (f32[256]{0:T(256)S(1)}, f32[256]{0:T(256)}, u32[]{:S(2)}) copy-start(f32[256]{0:T(256)} %param.19) | copy-start | bytes 3076
  50.8 4.9 %copy-start.7 = (bf16[128,256]{1,0:T(8,128)(2,1)S(1)}, bf16[128,256]{1,0:T(8,128)(2,1)}, u32[]{:S(2)}) copy-start(bf16[128,256]{1,0:T(8,128)(2,1)} %param.15) | copy-start | bytes 196612
  50.8 5.1 %copy-start.8 = (bf16[128,256]{1,0:T(8,128)(2,1)S(1)}, bf16[128,256]{1,0:T(8,128)(2,1)}, u32[]{:S(2)}) copy-start(bf16[128,256]{1,0:T(8,128)(2,1)} %param.17) | copy-start | bytes 196612
  50.8 54.5 %all-to-all-start.1 = ((bf16[4,704,128]{2,1,0:T(8,128)(2,1)}), bf16[4,704,128]{2,1,0:T(8,128)(2,1)S(1)}, u32[]{:S(2)}, u32[]{:S(2)}) async-start(bf16[4,704,128]{2,1,0:T(8,128)(2,1)} %bitcast.45), calls=%async_computation.1 | async-start | bytes 1441792 | tf_op jit(solution)/shard_map/all_to_all | solution.py:97
  54.5 124.0 %all-gather.18.cloned.1.call-start = ((), (), s32[]{:S(2)}) async-start(), calls=%async_computation.9 | async-start | bytes 3604480 | tf_op jit(solution)/shard_map/all_gather | solution.py:102
  55.8 37.1 %copy-start.9 = (f32[1024]{0:T(1024)S(1)}, f32[1024]{0:T(1024)}, u32[]{:S(2)}) copy-start(f32[1024]{0:T(1024)} %param.22) | copy-start | bytes 12292
  103.6 1.6 copy-start.11
  105.3 0.9 copy-start.2
  106.2 131.1 %reduce-scatter.3.cloned.1.call-start = ((), (), s32[]{:S(2)}) async-start(), calls=%async_computation.4 | async-start | bytes 2621440 | tf_op jit(solution)/shard_map/reduce_scatter | solution.py:201
  167.8 1.1 copy-start.3
  169.0 16.9 %collective-permute-start = (bf16[4,2,1408]{2,1,0:T(2,128)(2,1)S(1)}, bf16[4,2,1408]{2,1,0:T(2,128)(2,1)S(1)}, u32[]{:S(2)}, u32[]{:S(2)}) collective-permute-start(bf16[4,2,1408]{2,1,0:T(2,128)(2,1)S(1)} %slice.620), channel_id=1, source_target_pairs={{0,2},{2,4},{4,6},{6,0},{8,10},{10,12},{12,14},{14,8},{16,18},{18,... | collective-permute-start | bytes 67592 | tf_op jit(solution)/shard_map/ppermute | solution.py:185
  188.5 1.8 copy-start.1
  193.4 59.8 %copy-start = (bf16[512,1024]{1,0:T(8,128)(2,1)S(1)}, bf16[512,1024]{1,0:T(8,128)(2,1)}, u32[]{:S(2)}) copy-start(bf16[512,1024]{1,0:T(8,128)(2,1)} %param.21) | copy-start | bytes 3145732
  193.4 59.8 %copy-start.4 = (bf16[128,1024]{1,0:T(8,128)(2,1)S(1)}, bf16[128,1024]{1,0:T(8,128)(2,1)}, u32[]{:S(2)}) copy-start(bf16[128,1024]{1,0:T(8,128)(2,1)} %param.14) | copy-start | bytes 786436
  193.5 59.8 %reduce-scatter.5.cloned.1.call-start = ((), (), s32[]{:S(2)}) async-start(), calls=%async_computation.5 | async-start | bytes 786432 | tf_op jit(solution)/shard_map/reduce_scatter | solution.py:204
Sparse Core Ops, SparseCore 0:
  8.9 35.8 all-gather.11
  46.8 59.1 all-gather.13
  107.6 42.0 all-gather.15
  151.2 27.2 all-gather.17
  193.6 43.6 reduce-scatter.2
  239.3 13.8 reduce-scatter.4
where the time goes:
time: 263 us; the launch traced here: 262 us
  blocking collectives  113 us (43%)
  waiting for transfers between devices  69.7 us (27%)
  local copies, waits for them, and re-layouts  35.9 us (14%)
  matrix products  19.2 us (7%)
  between operations  14.4 us (5%)
  other arithmetic  5.76 us (2%)
  starting transfers between devices  3.9 us (1%)
    reduce_scatter x1, waiting for transfers between devices, on_device(): lax.psum_scatter(terms, 'sp', scatter_dimension=0, tiled=True, axis_index...  43.7 us
    all_to_all x1, blocking collectives, exchange(): lax.all_to_all(array, 'sp', 0, 0, axis_index_groups=outer_groups, tiled=T...  40.4 us
    all_gather x1, blocking collectives, on_device(): everyone = lax.all_gather(packed, 'sp').astype(f32)  35.8 us
    all_gather x1, blocking collectives, gather_wide(): lax.all_gather(array, ('sp', 'tp'), axis_index_groups=wide_groups)  32.7 us
    unnamed x71, local copies, waits for them, and re-layouts  18.5 us
    reduce_scatter x1, waiting for transfers between devices, on_device(): summed = lax.psum_scatter(summed, 'tp', scatter_dimension=1, tiled=True)  15.9 us
    all_gather x2, waiting for transfers between devices, gather_inner(): return lax.all_gather(array, 'sp', axis_index_groups=inner_groups)  8.49 us
    dot_general x1, matrix products, on_device(): up = jnp.dot(normed, up_chunk, preferred_element_type=f32).astype(bf16)  7.36 us
  transfers between devices with their start and end apart: 8, of which 3 were waited for; matrix products, arithmetic and copies ran while one was open for 19% of the time, Pallas kernels for 0%

commit v1 on v0

--- a/solution.py
+++ b/solution.py
@@ -1,14 +1,512 @@
+import functools
+
 import jax
 import jax.numpy as jnp
 from jax import lax
+from jax.experimental import pallas as pl
+from jax.experimental.pallas import tpu as pltpu
 from jax.sharding import PartitionSpec as P
 
 DK = 64
 SUB = 16
+LANES = 128
+INNER = 4
+OUTER = 4
 epsilon = 1e-06
 highest = lax.Precision.HIGHEST
 f32 = jnp.float32
 bf16 = jnp.bfloat16
+MESH = pl.DeviceIdType.MESH
+
+
+def dot_nt(a, b):
+    return lax.dot_general(
+        a, b, (((1,), (1,)), ((), ())), precision=highest, preferred_element_type=f32
+    )
+
+
+def dot_hi(a, b):
+    return jnp.dot(a, b, precision=highest, preferred_element_type=f32)
+
+
+def layer_kernel(
+    full,
+    extra,
+    up_in,
+    dn_in,
+    keys_ref,
+    logd_ref,
+    query_ref,
+    values_ref,
+    gating_ref,
+    head_gain_ref,
+    residual_ref,
+    out_weight_ref,
+    norm_gain_ref,
+    taps_ref,
+    out_ref,
+    up,
+    dn,
+    st,
+    zt,
+    inner_buf,
+    start_buf,
+    ho,
+    sq,
+    stream,
+    nb,
+    ubuf,
+    tail_s,
+    tail_r,
+    hid,
+    acc,
+    xs,
+    xr,
+    zs,
+    zr,
+    ssem,
+    up_r,
+    dn_r,
+    st_r,
+    zt_r,
+    nb_r,
+    xr_r,
+    zr_r,
+    misc_r,
+):
+    s = lax.axis_index("sp")
+    x = lax.axis_index("tp")
+    z = s // INNER
+    i = s % INNER
+    c = s % 2
+    ox = 1 - x
+    ic = i + 1 - 2 * c
+    iy = (i + 2) % INNER
+    idg = (ic + 2) % INNER
+    z1 = z + 1 - 2 * (z % 2)
+    z2 = (z + 2) % OUTER
+    z3 = OUTER - 1 - z
+    chunk = full + extra
+    rows = keys_ref.shape[0]
+    width = keys_ref.shape[1]
+    pairs = width // LANES
+    pending = []
+
+    def at(zz, ii, xx=x):
+        return {"sp": zz * INNER + ii, "tp": xx}
+
+    def send(src, dst, rsem, device):
+        copy = pltpu.make_async_remote_copy(
+            src_ref=src,
+            dst_ref=dst,
+            send_sem=ssem.at[len(pending)],
+            recv_sem=rsem,
+            device_id=device,
+            device_id_type=MESH,
+        )
+        copy.start()
+        pending.append(copy)
+
+    def arrived(dst, rsem):
+        pltpu.make_async_remote_copy(
+            src_ref=dst,
+            dst_ref=dst,
+            send_sem=ssem.at[0],
+            recv_sem=rsem,
+            device_id=at(z, ic),
+            device_id_type=MESH,
+        ).wait_recv()
+
+    barrier = pltpu.get_barrier_semaphore()
+    peers = [at((z + k) % OUTER, i) for k in range(1, OUTER)]
+    peers += [at(z, ic), at(z, iy), at(z, idg), at(z, i, ox)]
+    for peer in peers:
+        pl.semaphore_signal(barrier, inc=1, device_id=peer, device_id_type=MESH)
+    pl.semaphore_wait(barrier, len(peers))
+
+    def up_slot(zz, ii):
+        return up.at[zz * INNER + ii], up_r.at[zz * INNER + ii]
+
+    def dn_slot(zz, ii):
+        slot = dn.at[zz * INNER + ii, pl.ds(0, chunk)]
+        return slot, dn_r.at[zz * INNER + ii]
+
+    def send_z(source, slot, k):
+        dst, sem = slot(z, i)
+        send(source.at[(z + k) % OUTER], dst, sem, at((z + k) % OUTER, i))
+
+    def forward_yc(slot, zz, source=None):
+        dst, sem = slot(zz, i)
+        if source is None:
+            arrived(dst, sem)
+            source = dst
+        send(source, dst, sem, at(z, iy))
+        send(source, dst, sem, at(z, ic))
+
+    def forward_c(slot, zz):
+        dst, sem = slot(zz, iy)
+        arrived(dst, sem)
+        send(dst, dst, sem, at(z, ic))
+
+    send_z(up_in, up_slot, 2)
+
+    keys = keys_ref[...]
+    position = lax.broadcasted_iota(jnp.int32, (rows, rows), 0)
+    earlier = lax.broadcasted_iota(jnp.int32, (rows, rows), 1)
+    running = dot_hi((position >= earlier).astype(f32), logd_ref[...])
+    ending = running[rows - 1 : rows]
+    kept = keys * jnp.exp(ending - running)
+    turned = values_ref[...].T
+    low = lax.broadcasted_iota(jnp.int32, (1, LANES), 1) < DK
+    for p in range(pairs):
+        lanes = slice(p * LANES, (p + 1) * LANES)
+        both = dot_hi(turned[lanes], kept[:, lanes])
+        st[i, 0:DK, lanes] = jnp.where(low, both[:DK], both[DK:])
+    st[i, DK : DK + 8] = jnp.broadcast_to(jnp.exp(ending), (8, width))
+    for ii in (ic, iy, idg):
+        send(st.at[i], st.at[i], st_r.at[i], at(z, ii))
+    forward_yc(up_slot, z, up_in.at[z])
+    forward_yc(dn_slot, z, dn_in.at[z])
+
+    up[s] = up_in[z]
+    dn[s, 0:chunk] = dn_in[z]
+    spare = dn.shape[1] - chunk
+    if spare:
+        for b in range(INNER * OUTER):
+            dn[b, chunk:] = jnp.zeros((spare, dn.shape[2]), bf16)
+    start_buf[...] = query_ref[...] * jnp.exp(running)
+
+    for ii in (ic, iy, idg):
+        arrived(st.at[ii], st_r.at[ii])
+    total = jnp.zeros((DK, width), f32)
+    mine = jnp.zeros((DK, width), f32)
+    total_decay = jnp.ones((1, width), f32)
+    my_decay = jnp.ones((1, width), f32)
+    for j in range(INNER):
+        decay = st[j, DK : DK + 1]
+        fresh = st[j, 0:DK]
+        mine = jnp.where(j < i, mine * decay + fresh, mine)
+        my_decay = jnp.where(j < i, my_decay * decay, my_decay)
+        total = total * decay + fresh
+        total_decay = total_decay * decay
+    zt[z, 0:DK] = total
+    zt[z, DK : DK + 8] = jnp.broadcast_to(total_decay, (8, width))
+    for k in range(1, OUTER):
+        send(zt.at[z], zt.at[z], zt_r.at[z], at((z + k) % OUTER, i))
+    send_z(up_in, up_slot, 1)
+    send_z(up_in, up_slot, 3)
+
+    cells = [[] for _ in range(pairs)]
+    row_of = lax.broadcasted_iota(jnp.int32, (rows, width), 0)
+    column = lax.broadcasted_iota(jnp.int32, (2 * SUB, rows), 1)
+    stacked = lax.broadcasted_iota(jnp.int32, (2 * SUB, rows), 0) % SUB
+    for n in range(rows // SUB):
+        part = slice(n * SUB, (n + 1) * SUB)
+        middle = running[n * SUB + SUB // 2 - 1 : n * SUB + SUB // 2]
+        query_part = query_ref[part] * jnp.exp(running[part] - middle)
+        reach = jnp.where(row_of < (n + 1) * SUB, middle - running, -jnp.inf)
+        key_part = keys * jnp.exp(reach)
+        for p in range(pairs):
+            lanes = slice(p * LANES, (p + 1) * LANES)
+            piece = query_part[:, lanes]
+            piece = jnp.concatenate(
+                [jnp.where(low, piece, 0.0), jnp.where(low, 0.0, piece)], axis=0
+            )
+            score = dot_nt(piece, key_part[:, lanes])
+            score = jnp.where(stacked + n * SUB >= column, score, 0.0)
+            cells[p].append(score)
+    for p in range(pairs):
+        lanes = slice(p * LANES, (p + 1) * LANES)
+        scores = jnp.concatenate(
+            [cell[:SUB] for cell in cells[p]] + [cell[SUB:] for cell in cells[p]],
+            axis=0,
+        )
+        result = dot_hi(scores, values_ref[:, lanes])
+        inner_buf[:, lanes] = jnp.where(low, result[:rows], result[rows:])
+
+    for k in range(1, OUTER):
+        zz = (z + k) % OUTER
+        arrived(zt.at[zz], zt_r.at[zz])
+    entering = jnp.zeros((DK, width), f32)
+    for j in range(OUTER - 1):
+        entering = jnp.where(
+            j < z, entering * zt[j, DK : DK + 1] + zt[j, 0:DK], entering
+        )
+    entering = entering * my_decay + mine
+    same_head = (
+        lax.broadcasted_iota(jnp.int32, (LANES, LANES), 0) // DK
+        == lax.broadcasted_iota(jnp.int32, (LANES, LANES), 1) // DK
+    ).astype(f32)
+    for p in range(pairs):
+        lanes = slice(p * LANES, (p + 1) * LANES)
+        piece = entering[:, lanes]
+        piece = jnp.concatenate(
+            [jnp.where(low, piece, 0.0), jnp.where(low, 0.0, piece)], axis=0
+        )
+        recurrent = inner_buf[:, lanes] + dot_nt(start_buf[:, lanes], piece)
+        squares = dot_hi(recurrent * recurrent, same_head) * (1.0 / DK)
+        scaled = recurrent * lax.rsqrt(squares + epsilon) * head_gain_ref[:, lanes]
+        ho[x, :, lanes] = (scaled * gating_ref[:, lanes]).astype(bf16)
+    send(ho.at[x], ho.at[x], misc_r.at[0], at(z, i, ox))
+
+    forward_yc(up_slot, z2)
+    forward_c(up_slot, z)
+
+    arrived(ho.at[ox], misc_r.at[0])
+    heads = jnp.concatenate([ho[0], ho[1]], axis=1)
+    stream[...] = residual_ref[...].astype(f32) + jnp.dot(
+        heads, out_weight_ref[...], preferred_element_type=f32
+    )
+    partial = jnp.sum(stream[...] * stream[...], axis=1, keepdims=True)
+    sq[x] = jnp.broadcast_to(partial, (rows, LANES))
+    send(sq.at[x], sq.at[x], misc_r.at[1], at(z, i, ox))
+    forward_c(dn_slot, z)
+    arrived(sq.at[ox], misc_r.at[1])
+    channels = 2 * stream.shape[1]
+    mean = (sq[0][:, 0:1] + sq[1][:, 0:1]) * (1.0 / channels)
+    normed = stream[...] * lax.rsqrt(mean + epsilon) * norm_gain_ref[...]
+    nb[z, x] = normed.astype(bf16)
+
+    def nb_slot(zz, xx):
+        return nb.at[zz, xx], nb_r.at[zz * 2 + xx]
+
+    def share(zz, devices):
+        dst, sem = nb_slot(zz, x)
+        for device in devices:
+            send(dst, dst, sem, device)
+
+    share(z, [at(z2, i), at(z1, i), at(z, i, ox)])
+    for k in (2, 1, 3):
+        send_z(dn_in, dn_slot, k)
+
+    forward_yc(up_slot, (z + 1) % OUTER)
+    forward_yc(up_slot, (z + 3) % OUTER)
+    forward_c(up_slot, z2)
+    arrived(*nb_slot(z1, x))
+    share(z1, [at(z, i, ox)])
+    arrived(*nb_slot(z2, x))
+    share(z2, [at(z1, i), at(z, i, ox)])
+    forward_yc(dn_slot, z2)
+    forward_c(up_slot, (z + 1) % OUTER)
+    forward_c(up_slot, (z + 3) % OUTER)
+    arrived(*nb_slot(z3, x))
+    share(z3, [at(z, i, ox)])
+
+    for zz in range(OUTER):
+        arrived(*up_slot(zz, ic))
+        arrived(*up_slot(zz, idg))
+        arrived(*nb_slot(zz, ox))
+
+    forward_yc(dn_slot, (z + 1) % OUTER)
+
+    count = OUTER * rows
+    half = nb.shape[3]
+    deep = half // up.shape[1]
+    first = nb[:, 0].reshape(count, half)
+    second = nb[:, 1].reshape(count, half)
+    span = up.shape[2]
+    step = 2 * LANES
+    for low_lane in range(0, span, step):
+        lanes = slice(low_lane, min(span, low_lane + step))
+        size = lanes.stop - lanes.start
+        product = jnp.dot(
+            first, up[0:deep, :, lanes].reshape(half, size), preferred_element_type=f32
+        ) + jnp.dot(
+            second,
+            up[deep : 2 * deep, :, lanes].reshape(half, size),
+            preferred_element_type=f32,
+        )
+        ubuf[:, 8:, lanes] = (
+            product.astype(bf16).astype(f32).reshape(OUTER, rows, size)
+        )
+    for b in range(OUTER):
+        tail_s[2 * b : 2 * b + 2] = ubuf[b, rows + 6 : rows + 8]
+    after = z * INNER + (i + 1) % INNER
+    send(tail_s, tail_r, misc_r.at[2], {"sp": after, "tp": x})
+
+    forward_c(dn_slot, z2)
+    forward_yc(dn_slot, (z + 3) % OUTER)
+
+    arrived(tail_r, misc_r.at[2])
+    for b in range(OUTER):
+        wrapped = tail_r[2 * b - 2 : 2 * b] if b else jnp.zeros((2, span), f32)
+        ubuf[b, 6:8] = jnp.where(i == 0, wrapped, tail_r[2 * b : 2 * b + 2])
+
+    def conv(b, lanes):
+        return (
+            taps_ref[z, 0:1, lanes] * ubuf[b, pl.ds(6, rows), lanes]
+            + taps_ref[z, 1:2, lanes] * ubuf[b, pl.ds(7, rows), lanes]
+            + taps_ref[z, 2:3, lanes] * ubuf[b, pl.ds(8, rows), lanes]
+        )
+
+    def gate(v):
+        return v / (1.0 + jnp.exp(-v))
+
+    @pl.loop(0, OUTER)
+    def _(b):
+        for t in range(full // LANES):
+            lanes = slice(t * LANES, (t + 1) * LANES)
+            other = slice(full + t * LANES, full + (t + 1) * LANES)
+            hid[b, :, lanes] = (gate(conv(b, other)) * conv(b, lanes)).astype(bf16)
+        if extra:
+            mixed = conv(b, slice(2 * full, 2 * full + LANES))
+            turned_half = pltpu.roll(mixed, LANES // 2, 1)
+            last = jnp.where(low, gate(turned_half) * mixed, 0.0)
+            hid[b, :, full : full + LANES] = last.astype(bf16)
+
+    forward_c(dn_slot, (z + 1) % OUTER)
+    forward_c(dn_slot, (z + 3) % OUTER)
+    for zz in range(OUTER):
+        arrived(*dn_slot(zz, ic))
+        arrived(*dn_slot(zz, idg))
+
+    hidden = hid[...].reshape(count, hid.shape[2])
+
+    def columns(base, store):
+        for j in range(deep // 2):
+            weight = jnp.concatenate(
+                [dn[base + 2 * j], dn[base + 2 * j + 1]], axis=1
+            )
+            product = jnp.dot(hidden, weight, preferred_element_type=f32)
+            store(slice(j * step, (j + 1) * step), product.reshape(OUTER, rows, step))
+
+    def store_other(lanes, value):
+        xs[:, :, lanes] = value.astype(bf16)
+
+    def store_own(lanes, value):
+        acc[:, :, lanes] = value
+
+    columns(ox * deep, store_other)
+    for zz in (z3, z1, z2, z):
+        send(xs.at[zz], xr.at[zz], xr_r.at[zz], at(z, i, ox))
+    columns(x * deep, store_own)
+
+    def summed(zz):
+        arrived(xr.at[zz], xr_r.at[zz])
+        return acc[zz] + xr[zz].astype(f32)
+
+    zs[0] = summed(z3).astype(bf16)
+    send(zs.at[0], zr.at[0], zr_r.at[0], at(z1, i))
+    zs[1] = summed(z1).astype(bf16)
+    send(zs.at[1], zr.at[1], zr_r.at[1], at(z1, i))
+    partial_sum = summed(z2)
+    arrived(zr.at[0], zr_r.at[0])
+    zs[2] = (partial_sum + zr[0].astype(f32)).astype(bf16)
+    send(zs.at[2], zr.at[2], zr_r.at[2], at(z2, i))
+    own = summed(z)
+    arrived(zr.at[1], zr_r.at[1])
+    own = own + zr[1].astype(f32)
+    arrived(zr.at[2], zr_r.at[2])
+    out_ref[...] = (stream[...] + (own + zr[2].astype(f32))).astype(bf16)
+
+    for copy in pending:
+        copy.wait_send()
+
+
+def fused_layer(
+    residual_in,
+    query_pre,
+    forget_pre,
+    value_pre,
+    gate_pre,
+    floor_gap,
+    head_gain,
+    out_weight,
+    norm_gain,
+    value_weight,
+    gate_weight,
+    value_taps,
+    gate_taps,
+    down_weight,
+):
+    rows, my_width = residual_in.shape
+    depth, half = value_weight.shape
+    width = query_pre.shape[1]
+    blocks = INNER * OUTER
+    full = half // LANES // OUTER * LANES
+    extra = half // OUTER - full
+    chunk = full + extra
+    padded = full + (LANES if extra else 0)
+
+    def arrange(value, gate):
+        parts = []
+        for o in range(OUTER):
+            main = slice(o * full, (o + 1) * full)
+            rest = slice(OUTER * full + o * extra, OUTER * full + (o + 1) * extra)
+            pieces = [value[:, main], gate[:, main]]
+            if extra:
+                pieces += [value[:, rest], gate[:, rest]]
+            parts.append(jnp.concatenate(pieces, axis=1))
+        return jnp.stack(parts)
+
+    up_parts = arrange(value_weight, gate_weight)
+    taps = arrange(value_taps, gate_taps)
+    main = down_weight[: OUTER * full].reshape(OUTER, full, depth)
+    rest = down_weight[OUTER * full :].reshape(OUTER, extra, depth)
+    dn_parts = jnp.concatenate([main, rest], axis=1)
+    keys = floor_gap * jax.nn.sigmoid(-forget_pre.astype(f32))
+    log_decay = jnp.log1p(-keys)
+    query = jax.nn.silu(query_pre.astype(f32))
+    gating = jax.nn.silu(gate_pre.astype(f32))
+    values = value_pre.astype(f32)
+    gain = jnp.tile(head_gain, width // DK)[None]
+
+    dma = pltpu.SemaphoreType.DMA
+    vmem = pl.BlockSpec(memory_space=pltpu.VMEM)
+    span = 2 * chunk
+    return pl.pallas_call(
+        functools.partial(layer_kernel, full, extra),
+        out_shape=jax.ShapeDtypeStruct((rows, my_width), bf16),
+        in_specs=[vmem] * 12,
+        out_specs=vmem,
+        scratch_shapes=[
+            pltpu.VMEM((blocks, depth, span), bf16),
+            pltpu.VMEM((blocks, padded, depth), bf16),
+            pltpu.VMEM((INNER, DK + 8, width), f32),
+            pltpu.VMEM((OUTER, DK + 8, width), f32),
+            pltpu.VMEM((rows, width), f32),
+            pltpu.VMEM((rows, width), f32),
+            pltpu.VMEM((2, rows, width), bf16),
+            pltpu.VMEM((2, rows, LANES), f32),
+            pltpu.VMEM((rows, my_width), f32),
+            pltpu.VMEM((OUTER, 2, rows, my_width), bf16),
+            pltpu.VMEM((OUTER, rows + 8, span), f32),
+            pltpu.VMEM((2 * OUTER, span), f32),
+            pltpu.VMEM((2 * OUTER, span), f32),
+            pltpu.VMEM((OUTER, rows, padded), bf16),
+            pltpu.VMEM((OUTER, rows, my_width), f32),
+            pltpu.VMEM((OUTER, rows, my_width), bf16),
+            pltpu.VMEM((OUTER, rows, my_width), bf16),
+            pltpu.VMEM((3, rows, my_width), bf16),
+            pltpu.VMEM((3, rows, my_width), bf16),
+            dma((80,)),
+            dma((blocks,)),
+            dma((blocks,)),
+            dma((INNER,)),
+            dma((OUTER,)),
+            dma((2 * OUTER,)),
+            dma((OUTER,)),
+            dma((3,)),
+            dma((3,)),
+        ],
+        compiler_params=pltpu.CompilerParams(
+            collective_id=0, has_side_effects=True, vmem_limit_bytes=56 * 2**20
+        ),
+        name="layer",
+    )(
+        up_parts,
+        dn_parts,
+        keys,
+        log_decay,
+        query,
+        values,
+        gating,
+        gain,
+        residual_in,
+        out_weight,
+        norm_gain[None],
+        taps,
+    )
 
 
 def local_recurrence(query_pre, forget_pre, value_pre, floor_gap):
@@ -209,10 +707,28 @@
     return (own + summed.astype(f32)).astype(bf16)
 
 
+def fits(mesh, residual_in, query_pre, *arrays):
+    depth, half = arrays[7].shape
+    extra = half // OUTER % LANES
+    return (
+        mesh.shape["sp"] == INNER * OUTER
+        and mesh.shape["tp"] == 2
+        and depth == LANES
+        and residual_in.shape == (LANES, depth * INNER * OUTER // 2)
+        and query_pre.shape[1] % LANES == 0
+        and half % LANES == 0
+        and extra in (0, LANES // 2)
+    )
+
+
 def solution(mesh):
     rows = P(("grp", "sp"), "tp")
+
+    def layer(*arrays):
+        return (fused_layer if fits(mesh, *arrays) else on_device)(*arrays)
+
     return jax.shard_map(
-        on_device,
+        layer,
         mesh=mesh,
         in_specs=(
             rows,

time: 263 us -> 134 us (0.51)
  the two profiles are of different devices: /device:TPU:0 before, /device:TPU:27 now
where the time goes in v1:
time: 134 us; the launch traced here: 133 us
  Pallas kernels  121 us (90%)
  local copies, waits for them, and re-layouts  6.81 us (5%)
  other arithmetic  5.13 us (4%)
    pallas_call x1, Pallas kernels, fused_layer(): pl.pallas_call(functools.partial(layer_kernel, full, extra), out_shape=ja...  121 us

profile of v1, /device:TPU:27, one launch (start us, length us, event | category | flops | bytes accessed | tf_op | source)
XLA Modules:
  0.0 133.4 jit_solution(8640077192323174492)
XLA Ops:
  0.0 1.5 %fusion.8 = (bf16[128,640]{1,0:T(8,128)(2,1)S(1)}, bf16[128,640]{1,0:T(8,128)(2,1)S(1)}, bf16[128,640]{1,0:T(8,128)(2,1)S(1)}, bf16[128,640]{1,0:T(8,128)(2,1)S(...) fusion(bf16[128,2816]{1,0:T(8,128)(2,1)} %param.24, ...), kind=kLoop, calls=%fused_computation.17 | loop fusion | bytes 2621440 | tf_op jit(solution)/shard_map/slice | solution.py:436
  1.5 1.0 fusion.6
  2.5 0.1 concatenate.30
  2.6 0.1 concatenate.29
  2.7 0.1 concatenate.28
  2.8 0.1 concatenate.27
  2.9 1.3 pad_maximum_fusion.up_in
  4.3 0.0 slice-start
  4.3 0.0 slice-start.1
  4.3 0.0 copy-start
  4.3 0.0 copy-start.6
  4.3 0.0 copy-start.2
  4.3 0.0 copy-start.3
  4.3 0.0 copy-start.1
  4.3 0.0 copy-start.7
  4.3 0.0 copy-start.4
  4.3 0.0 copy-start.5
  4.4 0.8 slice-done
  5.1 0.3 slice-done.1
  5.4 0.9 pad_maximum_fusion.1.dn_in
  6.3 0.0 copy-done
  6.3 0.0 copy-done.6
  6.3 0.8 negate_log-plus-one_fusion
  7.1 0.0 copy-done.2
  7.1 0.0 copy-done.3
  7.1 0.8 convert_multiply_fusion
  7.9 0.0 copy-done.1
  7.9 0.7 convert_element_type.14.values_ref
  8.6 0.0 copy-done.7
  8.6 0.7 broadcast_in_dim_tile.3.head_gain_ref
  9.2 0.0 copy-done.4
  9.2 0.0 copy-done.5
  9.2 0.1 fusion.10
  9.3 0.1 concatenate.35
  9.4 0.1 concatenate.34
  9.5 0.1 concatenate.33
  9.6 0.1 concatenate.32
  9.7 0.7 pad_maximum_fusion.2.taps_ref
  10.4 121.3 %layer.1 = bf16[128,1024]{1,0:T(8,128)(2,1)} custom-call(bf16[4,128,1408]{2,1,0:T(8,128)(2,1)} %pad_maximum_fusion.up_in, bf16[4,704,128]{2,1,0:T(8,128)(2,1)} %pad_maximum_fusion.1.dn_in, f32[128,256]{1,0:T(8,128)} %get-tuple-element.22.keys_ref, f32[128,256]{1,0:T(8,128)} %get-tuple-element.21.logd_ref, f32[128,256]{1,0:T(8,128)} %get-tuple-element.56.query_ref, ...), custom_call_target="tpu_custom_call" | custom-call | tf_op jit(solution)/shard_map/layer/pallas_call | solution.py:457
  131.7 1.7 %copy.16 = bf16[128,1024]{1,0:T(8,128)(2,1)} copy(bf16[128,1024]{1,0:T(8,128)(2,1)} %layer.1) | data formatting | bytes 524288
  (2 shorter events, 0.0 us)
Async XLA Ops:
  4.3 0.8 slice-start
  4.3 1.1 slice-start.1
  4.3 2.0 %copy-start = (bf16[128,256]{1,0:T(8,128)(2,1)S(1)}, bf16[128,256]{1,0:T(8,128)(2,1)}, u32[]{:S(2)}) copy-start(bf16[128,256]{1,0:T(8,128)(2,1)} %param.16) | copy-start | bytes 196612
  4.3 2.0 %copy-start.6 = (f32[256]{0:T(256)S(1)}, f32[256]{0:T(256)}, u32[]{:S(2)}) copy-start(f32[256]{0:T(256)} %param.19) | copy-start | bytes 3076
  4.3 2.8 %copy-start.2 = (bf16[128,256]{1,0:T(8,128)(2,1)S(1)}, bf16[128,256]{1,0:T(8,128)(2,1)}, u32[]{:S(2)}) copy-start(bf16[128,256]{1,0:T(8,128)(2,1)} %param.18) | copy-start | bytes 196612
  4.3 2.8 %copy-start.3 = (bf16[128,256]{1,0:T(8,128)(2,1)S(1)}, bf16[128,256]{1,0:T(8,128)(2,1)}, u32[]{:S(2)}) copy-start(bf16[128,256]{1,0:T(8,128)(2,1)} %param.15) | copy-start | bytes 196612
  4.3 3.6 %copy-start.1 = (bf16[128,256]{1,0:T(8,128)(2,1)S(1)}, bf16[128,256]{1,0:T(8,128)(2,1)}, u32[]{:S(2)}) copy-start(bf16[128,256]{1,0:T(8,128)(2,1)} %param.17) | copy-start | bytes 196612
  4.3 4.2 %copy-start.7 = (f32[64]{0:T(128)S(1)}, f32[64]{0:T(128)}, u32[]{:S(2)}) copy-start(f32[64]{0:T(128)} %param.20) | copy-start | bytes 772
  4.3 4.9 %copy-start.4 = (f32[3,2816]{1,0:T(4,128)S(1)}, f32[3,2816]{1,0:T(4,128)}, u32[]{:S(2)}) copy-start(f32[3,2816]{1,0:T(4,128)} %param.26) | copy-start | bytes 101380
  4.3 4.9 %copy-start.5 = (f32[3,2816]{1,0:T(4,128)S(1)}, f32[3,2816]{1,0:T(4,128)}, u32[]{:S(2)}) copy-start(f32[3,2816]{1,0:T(4,128)} %param.25) | copy-start | bytes 101380

commit v2 on v1

--- a/solution.py
+++ b/solution.py
@@ -29,22 +29,35 @@
     return jnp.dot(a, b, precision=highest, preferred_element_type=f32)
 
 
+def gate(v):
+    return v / (1.0 + jnp.exp(-v))
+
+
+def turn(v):
+    return jnp.concatenate([v[:, DK:], v[:, :DK]], axis=1)
+
+
 def layer_kernel(
     full,
     extra,
+    residual_ref,
+    query_ref,
+    forget_ref,
+    value_ref,
+    gate_ref,
+    floor_ref,
+    head_gain_ref,
+    out_weight_ref,
+    norm_gain_ref,
+    value_weight_ref,
+    gate_weight_ref,
+    value_taps_ref,
+    gate_taps_ref,
+    down_ref,
+    out_ref,
     up_in,
     dn_in,
-    keys_ref,
-    logd_ref,
-    query_ref,
-    values_ref,
-    gating_ref,
-    head_gain_ref,
-    residual_ref,
-    out_weight_ref,
-    norm_gain_ref,
-    taps_ref,
-    out_ref,
+    taps,
     up,
     dn,
     st,
@@ -87,8 +100,8 @@
     z2 = (z + 2) % OUTER
     z3 = OUTER - 1 - z
     chunk = full + extra
-    rows = keys_ref.shape[0]
-    width = keys_ref.shape[1]
+    rows = query_ref.shape[0]
+    width = query_ref.shape[1]
     pairs = width // LANES
     pending = []
 
@@ -131,9 +144,9 @@
         slot = dn.at[zz * INNER + ii, pl.ds(0, chunk)]
         return slot, dn_r.at[zz * INNER + ii]
 
-    def send_z(source, slot, k):
+    def send_z(source, slot, zz):
         dst, sem = slot(z, i)
-        send(source.at[(z + k) % OUTER], dst, sem, at((z + k) % OUTER, i))
+        send(source.at[zz], dst, sem, at(zz, i))
 
     def forward_yc(slot, zz, source=None):
         dst, sem = slot(zz, i)
@@ -148,33 +161,67 @@
         arrived(dst, sem)
         send(dst, dst, sem, at(z, ic))
 
-    send_z(up_in, up_slot, 2)
-
-    keys = keys_ref[...]
+    keys = floor_ref[...] * jax.nn.sigmoid(-forget_ref[...].astype(f32))
+    query = gate(query_ref[...].astype(f32))
+    values = value_ref[...].astype(f32)
     position = lax.broadcasted_iota(jnp.int32, (rows, rows), 0)
     earlier = lax.broadcasted_iota(jnp.int32, (rows, rows), 1)
-    running = dot_hi((position >= earlier).astype(f32), logd_ref[...])
+    running = dot_hi((position >= earlier).astype(f32), jnp.log1p(-keys))
     ending = running[rows - 1 : rows]
     kept = keys * jnp.exp(ending - running)
-    turned = values_ref[...].T
+    turned = values.T
     low = lax.broadcasted_iota(jnp.int32, (1, LANES), 1) < DK
+    part_row = lax.broadcasted_iota(jnp.int32, (SUB, width), 0)
+
+    def store_state(ref, state, decay):
+        ref[0:DK] = state.astype(bf16)
+        one = decay.astype(bf16).astype(f32)
+        two = (decay - one).astype(bf16).astype(f32)
+        three = decay - one - two
+        parts = jnp.where(part_row == 1, two, jnp.where(part_row == 2, three, 0.0))
+        ref[DK : DK + SUB] = jnp.where(part_row == 0, one, parts).astype(bf16)
+
+    def load_state(ref):
+        parts = ref[DK : DK + SUB].astype(f32)
+        return ref[0:DK].astype(f32), parts[0:1] + parts[1:2] + parts[2:3]
+
+    states = []
     for p in range(pairs):
         lanes = slice(p * LANES, (p + 1) * LANES)
         both = dot_hi(turned[lanes], kept[:, lanes])
-        st[i, 0:DK, lanes] = jnp.where(low, both[:DK], both[DK:])
-    st[i, DK : DK + 8] = jnp.broadcast_to(jnp.exp(ending), (8, width))
+        states.append(jnp.where(low, both[:DK], both[DK:]))
+    store_state(st.at[i], jnp.concatenate(states, axis=1), jnp.exp(ending))
     for ii in (ic, iy, idg):
         send(st.at[i], st.at[i], st_r.at[i], at(z, ii))
+
+    for o in range(OUTER):
+        main = slice(o * full, (o + 1) * full)
+        up_in[o, :, 0:full] = value_weight_ref[:, main]
+        up_in[o, :, full : 2 * full] = gate_weight_ref[:, main]
+        dn_in[o, 0:full] = down_ref[main]
+        if extra:
+            start = OUTER * full + o * extra
+            dn_in[o, full:chunk] = down_ref[start : start + extra]
+    if extra:
+        for o in range(0, OUTER, 2):
+            start = OUTER * full + o * extra
+            tile = slice(start, start + LANES)
+            v = value_weight_ref[:, tile].astype(f32)
+            g = gate_weight_ref[:, tile].astype(f32)
+            end = slice(2 * full, 2 * full + LANES)
+            up_in[o, :, end] = jnp.where(low, v, turn(g)).astype(bf16)
+            up_in[o + 1, :, end] = jnp.where(low, turn(v), g).astype(bf16)
+
     forward_yc(up_slot, z, up_in.at[z])
+    send_z(dn_in, dn_slot, z1)
     forward_yc(dn_slot, z, dn_in.at[z])
-
     up[s] = up_in[z]
     dn[s, 0:chunk] = dn_in[z]
     spare = dn.shape[1] - chunk
     if spare:
         for b in range(INNER * OUTER):
             dn[b, chunk:] = jnp.zeros((spare, dn.shape[2]), bf16)
-    start_buf[...] = query_ref[...] * jnp.exp(running)
+    start_buf[...] = query * jnp.exp(running)
 
     for ii in (ic, iy, idg):
         arrived(st.at[ii], st_r.at[ii])
@@ -183,18 +230,16 @@
     total_decay = jnp.ones((1, width), f32)
     my_decay = jnp.ones((1, width), f32)
     for j in range(INNER):
-        decay = st[j, DK : DK + 1]
-        fresh = st[j, 0:DK]
+        fresh, decay = load_state(st.at[j])
         mine = jnp.where(j < i, mine * decay + fresh, mine)
         my_decay = jnp.where(j < i, my_decay * decay, my_decay)
         total = total * decay + fresh
         total_decay = total_decay * decay
-    zt[z, 0:DK] = total
-    zt[z, DK : DK + 8] = jnp.broadcast_to(total_decay, (8, width))
+    store_state(zt.at[z], total, total_decay)
     for k in range(1, OUTER):
         send(zt.at[z], zt.at[z], zt_r.at[z], at((z + k) % OUTER, i))
-    send_z(up_in, up_slot, 1)
-    send_z(up_in, up_slot, 3)
+    send_z(up_in, up_slot, z2)
+    send_z(up_in, up_slot, z1)
 
     cells = [[] for _ in range(pairs)]
     row_of = lax.broadcasted_iota(jnp.int32, (rows, width), 0)
@@ -203,7 +248,7 @@
     for n in range(rows // SUB):
         part = slice(n * SUB, (n + 1) * SUB)
         middle = running[n * SUB + SUB // 2 - 1 : n * SUB + SUB // 2]
-        query_part = query_ref[part] * jnp.exp(running[part] - middle)
+        query_part = query[part] * jnp.exp(running[part] - middle)
         reach = jnp.where(row_of < (n + 1) * SUB, middle - running, -jnp.inf)
         key_part = keys * jnp.exp(reach)
         for p in range(pairs):
@@ -221,17 +266,18 @@
             [cell[:SUB] for cell in cells[p]] + [cell[SUB:] for cell in cells[p]],
             axis=0,
         )
-        result = dot_hi(scores, values_ref[:, lanes])
+        result = dot_hi(scores, values[:, lanes])
         inner_buf[:, lanes] = jnp.where(low, result[:rows], result[rows:])
 
+    gain = jnp.concatenate([head_gain_ref[...]] * (LANES // DK), axis=1)
+    gating = gate(gate_ref[...].astype(f32))
     for k in range(1, OUTER):
         zz = (z + k) % OUTER
         arrived(zt.at[zz], zt_r.at[zz])
     entering = jnp.zeros((DK, width), f32)
     for j in range(OUTER - 1):
-        entering = jnp.where(
-            j < z, entering * zt[j, DK : DK + 1] + zt[j, 0:DK], entering
-        )
+        fresh, decay = load_state(zt.at[j])
+        entering = jnp.where(j < z, entering * decay + fresh, entering)
     entering = entering * my_decay + mine
     same_head = (
         lax.broadcasted_iota(jnp.int32, (LANES, LANES), 0) // DK
@@ -245,11 +291,10 @@
         )
         recurrent = inner_buf[:, lanes] + dot_nt(start_buf[:, lanes], piece)
         squares = dot_hi(recurrent * recurrent, same_head) * (1.0 / DK)
-        scaled = recurrent * lax.rsqrt(squares + epsilon) * head_gain_ref[:, lanes]
-        ho[x, :, lanes] = (scaled * gating_ref[:, lanes]).astype(bf16)
+        scaled = recurrent * lax.rsqrt(squares + epsilon) * gain
+        ho[x, :, lanes] = (scaled * gating[:, lanes]).astype(bf16)
     send(ho.at[x], ho.at[x], misc_r.at[0], at(z, i, ox))
 
-    forward_yc(up_slot, z2)
     forward_c(up_slot, z)
 
     arrived(ho.at[ox], misc_r.at[0])
@@ -260,7 +305,6 @@
     partial = jnp.sum(stream[...] * stream[...], axis=1, keepdims=True)
     sq[x] = jnp.broadcast_to(partial, (rows, LANES))
     send(sq.at[x], sq.at[x], misc_r.at[1], at(z, i, ox))
-    forward_c(dn_slot, z)
     arrived(sq.at[ox], misc_r.at[1])
     channels = 2 * stream.shape[1]
     mean = (sq[0][:, 0:1] + sq[1][:, 0:1]) * (1.0 / channels)
@@ -276,28 +320,40 @@
             send(dst, dst, sem, device)
 
     share(z, [at(z2, i), at(z1, i), at(z, i, ox)])
-    for k in (2, 1, 3):
-        send_z(dn_in, dn_slot, k)
-
-    forward_yc(up_slot, (z + 1) % OUTER)
-    forward_yc(up_slot, (z + 3) % OUTER)
-    forward_c(up_slot, z2)
+    forward_c(dn_slot, z)
+    forward_yc(up_slot, z2)
+    forward_yc(up_slot, z1)
+    arrived(*nb_slot(z2, x))
+    share(z2, [at(z1, i), at(z, i, ox)])
+    send_z(up_in, up_slot, z3)
     arrived(*nb_slot(z1, x))
     share(z1, [at(z, i, ox)])
-    arrived(*nb_slot(z2, x))
-    share(z2, [at(z1, i), at(z, i, ox)])
-    forward_yc(dn_slot, z2)
-    forward_c(up_slot, (z + 1) % OUTER)
-    forward_c(up_slot, (z + 3) % OUTER)
+    forward_c(up_slot, z2)
+    forward_c(up_slot, z1)
+    forward_yc(dn_slot, z1)
     arrived(*nb_slot(z3, x))
     share(z3, [at(z, i, ox)])
+    forward_yc(up_slot, z3)
+    forward_c(dn_slot, z1)
+    forward_c(up_slot, z3)
+    send_z(dn_in, dn_slot, z2)
+    send_z(dn_in, dn_slot, z3)
 
     for zz in range(OUTER):
         arrived(*up_slot(zz, ic))
         arrived(*up_slot(zz, idg))
         arrived(*nb_slot(zz, ox))
 
-    forward_yc(dn_slot, (z + 1) % OUTER)
+    mine_at = pl.ds(pl.multiple_of(z * full, LANES), full)
+    taps[:, 0:full] = value_taps_ref[:, mine_at]
+    taps[:, full : 2 * full] = gate_taps_ref[:, mine_at]
+    if extra:
+        tile = pl.ds(pl.multiple_of(OUTER * full + z // 2 * LANES, LANES), LANES)
+        v = value_taps_ref[:, tile]
+        g = gate_taps_ref[:, tile]
+        v = jnp.where(z % 2 == 0, v, turn(v))
+        g = jnp.where(z % 2 == 0, turn(g), g)
+        taps[:, 2 * full : 2 * full + LANES] = jnp.where(low, v, g)
 
     count = OUTER * rows
     half = nb.shape[3]
@@ -324,8 +380,8 @@
     after = z * INNER + (i + 1) % INNER
     send(tail_s, tail_r, misc_r.at[2], {"sp": after, "tp": x})
 
-    forward_c(dn_slot, z2)
-    forward_yc(dn_slot, (z + 3) % OUTER)
+    forward_yc(dn_slot, z2)
+    forward_yc(dn_slot, z3)
 
     arrived(tail_r, misc_r.at[2])
     for b in range(OUTER):
@@ -334,13 +390,10 @@
 
     def conv(b, lanes):
         return (
-            taps_ref[z, 0:1, lanes] * ubuf[b, pl.ds(6, rows), lanes]
-            + taps_ref[z, 1:2, lanes] * ubuf[b, pl.ds(7, rows), lanes]
-            + taps_ref[z, 2:3, lanes] * ubuf[b, pl.ds(8, rows), lanes]
+            taps[0:1, lanes] * ubuf[b, pl.ds(6, rows), lanes]
+            + taps[1:2, lanes] * ubuf[b, pl.ds(7, rows), lanes]
+            + taps[2:3, lanes] * ubuf[b, pl.ds(8, rows), lanes]
         )
-
-    def gate(v):
-        return v / (1.0 + jnp.exp(-v))
 
     @pl.loop(0, OUTER)
     def _(b):
@@ -350,36 +403,29 @@
             hid[b, :, lanes] = (gate(conv(b, other)) * conv(b, lanes)).astype(bf16)
         if extra:
             mixed = conv(b, slice(2 * full, 2 * full + LANES))
-            turned_half = pltpu.roll(mixed, LANES // 2, 1)
+            turned_half = turn(mixed)
             last = jnp.where(low, gate(turned_half) * mixed, 0.0)
             hid[b, :, full : full + LANES] = last.astype(bf16)
 
-    forward_c(dn_slot, (z + 1) % OUTER)
-    forward_c(dn_slot, (z + 3) % OUTER)
+    forward_c(dn_slot, z2)
+    forward_c(dn_slot, z3)
     for zz in range(OUTER):
         arrived(*dn_slot(zz, ic))
         arrived(*dn_slot(zz, idg))
 
-    hidden = hid[...].reshape(count, hid.shape[2])
-
-    def columns(base, store):
+    def columns(zz, base, store):
         for j in range(deep // 2):
             weight = jnp.concatenate(
                 [dn[base + 2 * j], dn[base + 2 * j + 1]], axis=1
             )
-            product = jnp.dot(hidden, weight, preferred_element_type=f32)
-            store(slice(j * step, (j + 1) * step), product.reshape(OUTER, rows, step))
-
-    def store_other(lanes, value):
-        xs[:, :, lanes] = value.astype(bf16)
-
-    def store_own(lanes, value):
-        acc[:, :, lanes] = value
-
-    columns(ox * deep, store_other)
+            product = jnp.dot(hid[zz], weight, preferred_element_type=f32)
+            store[zz, :, j * step : (j + 1) * step] = product.astype(store.dtype)
+
     for zz in (z3, z1, z2, z):
+        columns(zz, ox * deep, xs)
         send(xs.at[zz], xr.at[zz], xr_r.at[zz], at(z, i, ox))
-    columns(x * deep, store_own)
+    for zz in (z3, z1, z2, z):
+        columns(zz, x * deep, acc)
 
     def summed(zz):
         arrived(xr.at[zz], xr_r.at[zz])
@@ -428,42 +474,22 @@
     chunk = full + extra
     padded = full + (LANES if extra else 0)
 
-    def arrange(value, gate):
-        parts = []
-        for o in range(OUTER):
-            main = slice(o * full, (o + 1) * full)
-            rest = slice(OUTER * full + o * extra, OUTER * full + (o + 1) * extra)
-            pieces = [value[:, main], gate[:, main]]
-            if extra:
-                pieces += [value[:, rest], gate[:, rest]]
-            parts.append(jnp.concatenate(pieces, axis=1))
-        return jnp.stack(parts)
-
-    up_parts = arrange(value_weight, gate_weight)
-    taps = arrange(value_taps, gate_taps)
-    main = down_weight[: OUTER * full].reshape(OUTER, full, depth)
-    rest = down_weight[OUTER * full :].reshape(OUTER, extra, depth)
-    dn_parts = jnp.concatenate([main, rest], axis=1)
-    keys = floor_gap * jax.nn.sigmoid(-forget_pre.astype(f32))
-    log_decay = jnp.log1p(-keys)
-    query = jax.nn.silu(query_pre.astype(f32))
-    gating = jax.nn.silu(gate_pre.astype(f32))
-    values = value_pre.astype(f32)
-    gain = jnp.tile(head_gain, width // DK)[None]
-
     dma = pltpu.SemaphoreType.DMA
     vmem = pl.BlockSpec(memory_space=pltpu.VMEM)
     span = 2 * chunk
     return pl.pallas_call(
         functools.partial(layer_kernel, full, extra),
         out_shape=jax.ShapeDtypeStruct((rows, my_width), bf16),
-        in_specs=[vmem] * 12,
+        in_specs=[vmem] * 14,
         out_specs=vmem,
         scratch_shapes=[
+            pltpu.VMEM((OUTER, depth, span), bf16),
+            pltpu.VMEM((OUTER, chunk, depth), bf16),
+            pltpu.VMEM((value_taps.shape[0], span), f32),
             pltpu.VMEM((blocks, depth, span), bf16),
             pltpu.VMEM((blocks, padded, depth), bf16),
-            pltpu.VMEM((INNER, DK + 8, width), f32),
-            pltpu.VMEM((OUTER, DK + 8, width), f32),
+            pltpu.VMEM((INNER, DK + SUB, width), bf16),
+            pltpu.VMEM((OUTER, DK + SUB, width), bf16),
             pltpu.VMEM((rows, width), f32),
             pltpu.VMEM((rows, width), f32),
             pltpu.VMEM((2, rows, width), bf16),
@@ -494,18 +520,20 @@
         ),
         name="layer",
     )(
-        up_parts,
-        dn_parts,
-        keys,
-        log_decay,
-        query,
-        values,
-        gating,
-        gain,
         residual_in,
+        query_pre,
+        forget_pre,
+        value_pre,
+        gate_pre,
+        floor_gap[None],
+        head_gain[None],
         out_weight,
         norm_gain[None],
-        taps,
+        value_weight,
+        gate_weight,
+        value_taps,
+        gate_taps,
+        down_weight,
     )
 
 

time: 134 us -> 122 us (0.910)
  the two profiles are of different devices: /device:TPU:27 before, /device:TPU:0 now
where the time goes in v2:
time: 122 us
  Pallas kernels  120 us (98%)
  local copies, waits for them, and re-layouts  1.67 us (1%)
    pallas_call x1, Pallas kernels, fused_layer(): pl.pallas_call(functools.partial(layer_kernel, full, extra), out_shape=ja...  120 us

profile of v2, /device:TPU:0, one launch (start us, length us, event | category | flops | bytes accessed | tf_op | source)
XLA Modules:
  0.0 121.8 jit_solution(17276925868638801494)
XLA Ops:
  0.0 120.1 %layer.1 = bf16[128,1024]{1,0:T(8,128)(2,1)} custom-call(bf16[128,1024]{1,0:T(8,128)(2,1)} %residual_ref.1, bf16[128,256]{1,0:T(8,128)(2,1)} %query_ref.1, bf16[128,256]{1,0:T(8,128)(2,1)} %forget_ref.1, bf16[128,256]{1,0:T(8,128)(2,1)} %value_ref.1, bf16[128,256]{1,0:T(8,128)(2,1)} %gate_ref.1, f32[1,256]{1,0:T(1,128)} %bitcast.4, f32[1,64]{1,0:T(1,128)} %bitcast.5, ...), custom_call_target="tpu_custom_call" | custom-call | tf_op jit(solution)/shard_map/layer/pallas_call | solution.py:480
  120.1 1.7 %copy.16 = bf16[128,1024]{1,0:T(8,128)(2,1)} copy(bf16[128,1024]{1,0:T(8,128)(2,1)} %layer.1) | data formatting | bytes 524288

commit v3 on v2

--- a/solution.py
+++ b/solution.py
@@ -82,6 +82,8 @@
     dn_r,
     st_r,
     zt_r,
+    zt_s,
+    go,
     nb_r,
     xr_r,
     zr_r,
@@ -100,6 +102,7 @@
     z2 = (z + 2) % OUTER
     z3 = OUTER - 1 - z
     chunk = full + extra
+    depth = up.shape[1]
     rows = query_ref.shape[0]
     width = query_ref.shape[1]
     pairs = width // LANES
@@ -108,7 +111,7 @@
     def at(zz, ii, xx=x):
         return {"sp": zz * INNER + ii, "tp": xx}
 
-    def send(src, dst, rsem, device):
+    def send(src, dst, rsem, device, first=None):
         copy = pltpu.make_async_remote_copy(
             src_ref=src,
             dst_ref=dst,
@@ -117,8 +120,12 @@
             device_id=device,
             device_id_type=MESH,
         )
-        copy.start()
         pending.append(copy)
+        if first is None:
+            copy.start()
+        elif first is not False:
+            pl.when(first)(copy.start)
+        return copy
 
     def arrived(dst, rsem):
         pltpu.make_async_remote_copy(
@@ -135,7 +142,6 @@
     peers += [at(z, ic), at(z, iy), at(z, idg), at(z, i, ox)]
     for peer in peers:
         pl.semaphore_signal(barrier, inc=1, device_id=peer, device_id_type=MESH)
-    pl.semaphore_wait(barrier, len(peers))
 
     def up_slot(zz, ii):
         return up.at[zz * INNER + ii], up_r.at[zz * INNER + ii]
@@ -144,9 +150,9 @@
         slot = dn.at[zz * INNER + ii, pl.ds(0, chunk)]
         return slot, dn_r.at[zz * INNER + ii]
 
-    def send_z(source, slot, zz):
+    def send_z(source, slot, zz, first=None):
         dst, sem = slot(z, i)
-        send(source.at[zz], dst, sem, at(zz, i))
+        return send(source.at[zz], dst, sem, at(zz, i), first)
 
     def forward_yc(slot, zz, source=None):
         dst, sem = slot(zz, i)
@@ -155,6 +161,17 @@
             source = dst
         send(source, dst, sem, at(z, iy))
         send(source, dst, sem, at(z, ic))
+
+    def prepare_yc(slot, zz):
+        dst, sem = slot(zz, i)
+        copies = [send(dst, dst, sem, at(z, ii), False) for ii in (iy, ic)]
+
+        def run():
+            arrived(dst, sem)
+            for copy in copies:
+                copy.start()
+
+        return run
 
     def forward_c(slot, zz):
         dst, sem = slot(zz, iy)
@@ -191,9 +208,6 @@
         both = dot_hi(turned[lanes], kept[:, lanes])
         states.append(jnp.where(low, both[:DK], both[DK:]))
     store_state(st.at[i], jnp.concatenate(states, axis=1), jnp.exp(ending))
-    for ii in (ic, iy, idg):
-        send(st.at[i], st.at[i], st_r.at[i], at(z, ii))
-
     for o in range(OUTER):
         main = slice(o * full, (o + 1) * full)
         up_in[o, :, 0:full] = value_weight_ref[:, main]
@@ -212,9 +226,14 @@
             up_in[o, :, end] = jnp.where(low, v, turn(g)).astype(bf16)
             up_in[o + 1, :, end] = jnp.where(low, turn(v), g).astype(bf16)
 
-    forward_yc(up_slot, z, up_in.at[z])
-    send_z(dn_in, dn_slot, z1)
-    forward_yc(dn_slot, z, dn_in.at[z])
+    pl.semaphore_wait(barrier, len(peers))
+    for ii in (idg, iy, ic):
+        send(st.at[i], st.at[i], st_r.at[i], at(z, ii))
+    far = send_z(up_in, up_slot, z2, z == 3)
+    near = send_z(up_in, up_slot, z1, z % 2 == 1)
+    near_dn = send_z(dn_in, dn_slot, z1, z % 2 == 0)
+    last_dn = send_z(dn_in, dn_slot, z3, z == 1)
+
     up[s] = up_in[z]
     dn[s, 0:chunk] = dn_in[z]
     spare = dn.shape[1] - chunk
@@ -236,10 +255,23 @@
         total = total * decay + fresh
         total_decay = total_decay * decay
     store_state(zt.at[z], total, total_decay)
+    totals = []
     for k in range(1, OUTER):
-        send(zt.at[z], zt.at[z], zt_r.at[z], at((z + k) % OUTER, i))
-    send_z(up_in, up_slot, z2)
-    send_z(up_in, up_slot, z1)
+        totals.append(
+            pltpu.make_async_remote_copy(
+                src_ref=zt.at[z],
+                dst_ref=zt.at[z],
+                send_sem=zt_s.at[k],
+                recv_sem=zt_r.at[z],
+                device_id=at((z + k) % OUTER, i),
+                device_id_type=MESH,
+            )
+        )
+    for k in (3, 2, 1):
+        pl.when(z + k < OUTER)(totals[k - 1].start)
+    pl.when(z == 2)(near.start)
+    forward_yc(up_slot, z, up_in.at[z])
+    forward_yc(dn_slot, z, dn_in.at[z])
 
     cells = [[] for _ in range(pairs)]
     row_of = lax.broadcasted_iota(jnp.int32, (rows, width), 0)
@@ -269,11 +301,19 @@
         result = dot_hi(scores, values[:, lanes])
         inner_buf[:, lanes] = jnp.where(low, result[:rows], result[rows:])
 
+    for k, copy in enumerate(totals, 1):
+        pl.when(z + k < OUTER)(copy.wait_send)
+
+    @pl.when(z == 1)
+    def _():
+        pl.semaphore_signal(go, inc=1, device_id=at(z1, i), device_id_type=MESH)
+
+    pl.when(z == 2)(far.start)
     gain = jnp.concatenate([head_gain_ref[...]] * (LANES // DK), axis=1)
     gating = gate(gate_ref[...].astype(f32))
     for k in range(1, OUTER):
-        zz = (z + k) % OUTER
-        arrived(zt.at[zz], zt_r.at[zz])
+        zz = (z + OUTER - k) % OUTER
+        pl.when(z >= k)(functools.partial(arrived, zt.at[zz], zt_r.at[zz]))
     entering = jnp.zeros((DK, width), f32)
     for j in range(OUTER - 1):
         fresh, decay = load_state(zt.at[j])
@@ -295,9 +335,14 @@
         ho[x, :, lanes] = (scaled * gating[:, lanes]).astype(bf16)
     send(ho.at[x], ho.at[x], misc_r.at[0], at(z, i, ox))
 
-    forward_c(up_slot, z)
+    @pl.when(z == 0)
+    def _():
+        pl.semaphore_wait(go, 1)
+        far.start()
+
 
     arrived(ho.at[ox], misc_r.at[0])
+    pl.when(z == 1)(far.start)
     heads = jnp.concatenate([ho[0], ho[1]], axis=1)
     stream[...] = residual_ref[...].astype(f32) + jnp.dot(
         heads, out_weight_ref[...], preferred_element_type=f32
@@ -314,30 +359,44 @@
     def nb_slot(zz, xx):
         return nb.at[zz, xx], nb_r.at[zz * 2 + xx]
 
-    def share(zz, devices):
+    def share(zz, devices, first=None):
         dst, sem = nb_slot(zz, x)
-        for device in devices:
-            send(dst, dst, sem, device)
+        return [send(dst, dst, sem, device, first) for device in devices]
 
     share(z, [at(z2, i), at(z1, i), at(z, i, ox)])
+    pl.when(z == 0)(near.start)
+    cross = send_z(up_in, up_slot, z3, z > 0)
+    pl.when(z % 2 == 1)(near_dn.start)
+    forward_c(up_slot, z)
     forward_c(dn_slot, z)
+    early_dn = prepare_yc(dn_slot, z1)
+    pl.when(z % 2 == 1)(early_dn)
     forward_yc(up_slot, z2)
-    forward_yc(up_slot, z1)
-    arrived(*nb_slot(z2, x))
-    share(z2, [at(z1, i), at(z, i, ox)])
-    send_z(up_in, up_slot, z3)
+
+    pl.when(z == 1)(functools.partial(arrived, *nb_slot(z2, x)))
+    passed = share(z2, [at(z1, i), at(z, i, ox)], z == 1)
     arrived(*nb_slot(z1, x))
     share(z1, [at(z, i, ox)])
+
+    @pl.when(z != 1)
+    def _():
+        arrived(*nb_slot(z2, x))
+        for copy in passed:
+            copy.start()
+
+    forward_yc(up_slot, z1)
     forward_c(up_slot, z2)
-    forward_c(up_slot, z1)
-    forward_yc(dn_slot, z1)
     arrived(*nb_slot(z3, x))
     share(z3, [at(z, i, ox)])
+    pl.when(z == 0)(cross.start)
+    forward_c(up_slot, z1)
     forward_yc(up_slot, z3)
-    forward_c(dn_slot, z1)
+    send_z(dn_in, dn_slot, z2)
+    pl.when(z % 2 == 0)(early_dn)
+    later_dn = prepare_yc(dn_slot, z2)
+    pl.when(z % 3 == 0)(later_dn)
     forward_c(up_slot, z3)
-    send_z(dn_in, dn_slot, z2)
-    send_z(dn_in, dn_slot, z3)
+    pl.when(z != 1)(last_dn.start)
 
     for zz in range(OUTER):
         arrived(*up_slot(zz, ic))
@@ -380,7 +439,8 @@
     after = z * INNER + (i + 1) % INNER
     send(tail_s, tail_r, misc_r.at[2], {"sp": after, "tp": x})
 
-    forward_yc(dn_slot, z2)
+    forward_c(dn_slot, z1)
+    pl.when(z % 3 != 0)(later_dn)
     forward_yc(dn_slot, z3)
 
     arrived(tail_r, misc_r.at[2])
@@ -413,39 +473,59 @@
         arrived(*dn_slot(zz, ic))
         arrived(*dn_slot(zz, idg))
 
-    def columns(zz, base, store):
-        for j in range(deep // 2):
+    def columns(zz, base, store, part):
+        each = deep // 4
+        for j in range(part * each, (part + 1) * each):
             weight = jnp.concatenate(
                 [dn[base + 2 * j], dn[base + 2 * j + 1]], axis=1
             )
             product = jnp.dot(hid[zz], weight, preferred_element_type=f32)
             store[zz, :, j * step : (j + 1) * step] = product.astype(store.dtype)
 
-    for zz in (z3, z1, z2, z):
-        columns(zz, ox * deep, xs)
-        send(xs.at[zz], xr.at[zz], xr_r.at[zz], at(z, i, ox))
-    for zz in (z3, z1, z2, z):
-        columns(zz, x * deep, acc)
-
-    def summed(zz):
-        arrived(xr.at[zz], xr_r.at[zz])
-        return acc[zz] + xr[zz].astype(f32)
-
-    zs[0] = summed(z3).astype(bf16)
-    send(zs.at[0], zr.at[0], zr_r.at[0], at(z1, i))
-    zs[1] = summed(z1).astype(bf16)
-    send(zs.at[1], zr.at[1], zr_r.at[1], at(z1, i))
-    partial_sum = summed(z2)
-    arrived(zr.at[0], zr_r.at[0])
-    zs[2] = (partial_sum + zr[0].astype(f32)).astype(bf16)
-    send(zs.at[2], zr.at[2], zr_r.at[2], at(z2, i))
-    own = summed(z)
-    arrived(zr.at[1], zr_r.at[1])
-    own = own + zr[1].astype(f32)
-    arrived(zr.at[2], zr_r.at[2])
-    out_ref[...] = (stream[...] + (own + zr[2].astype(f32))).astype(bf16)
-
-    for copy in pending:
+    sides = [slice(0, half // 2), slice(half // 2, half)]
+
+    def send_part(src, dst, sem, slot, part, device):
+        side = sides[part]
+        send(src.at[slot, :, side], dst.at[slot, :, side], sem.at[slot, part], device)
+
+    phase = len(pending)
+    order = [(z3, 0), (z2, 0), (z3, 1), (z2, 1), (z1, 0), (z1, 1), (z, 0), (z, 1)]
+    for zz, part in order:
+        columns(zz, ox * deep, xs, part)
+        send_part(xs, xr, xr_r, zz, part, at(z, i, ox))
+
+    for copy in pending[:phase]:
+        copy.wait_send()
+
+    def summed(zz, part):
+        side = sides[part]
+        columns(zz, x * deep, acc, part)
+        arrived(xr.at[zz, :, side], xr_r.at[zz, part])
+        return acc[zz, :, side] + xr[zz, :, side].astype(f32)
+
+    def received(slot, part):
+        side = sides[part]
+        arrived(zr.at[slot, :, side], zr_r.at[slot, part])
+        return zr[slot, :, side].astype(f32)
+
+    def pass_on(slot, part, value, device):
+        zs[slot, :, sides[part]] = value.astype(bf16)
+        send_part(zs, zr, zr_r, slot, part, device)
+
+    pass_on(0, 0, summed(z3, 0), at(z1, i))
+    value = summed(z2, 0)
+    pass_on(2, 0, value + received(0, 0), at(z2, i))
+    pass_on(0, 1, summed(z3, 1), at(z1, i))
+    value = summed(z2, 1)
+    pass_on(2, 1, value + received(0, 1), at(z2, i))
+    for part in range(2):
+        pass_on(1, part, summed(z1, part), at(z1, i))
+    for part in range(2):
+        side = sides[part]
+        own = summed(z, part) + received(1, part) + received(2, part)
+        out_ref[:, side] = (stream[:, side] + own).astype(bf16)
+
+    for copy in pending[phase:]:
         copy.wait_send()
 
 
@@ -510,9 +590,11 @@
             dma((blocks,)),
             dma((INNER,)),
             dma((OUTER,)),
+            dma((OUTER,)),
+            pltpu.SemaphoreType.REGULAR,
             dma((2 * OUTER,)),
-            dma((OUTER,)),
-            dma((3,)),
+            dma((OUTER, 2)),
+            dma((3, 2)),
             dma((3,)),
         ],
         compiler_params=pltpu.CompilerParams(

time: 122 us -> 114 us (0.934)
  Pallas kernels: 120 us -> 112 us
    pallas_call x1, Pallas kernels: 120 us -> 112 us  [fused_layer(): pl.pallas_call(functools.partial(layer_kernel, full, extra), out_shape=ja...]
where the time goes in v3:
time: 114 us; the launch traced here: 113 us
  Pallas kernels  112 us (98%)
  local copies, waits for them, and re-layouts  1.67 us (1%)
    pallas_call x1, Pallas kernels, fused_layer(): pl.pallas_call(functools.partial(layer_kernel, full, extra), out_shape=ja...  112 us

profile of v3, /device:TPU:0, one launch (start us, length us, event | category | flops | bytes accessed | tf_op | source)
XLA Modules:
  0.0 113.2 jit_solution(16580934060444427465)
XLA Ops:
  0.0 111.6 %layer.1 = bf16[128,1024]{1,0:T(8,128)(2,1)} custom-call(bf16[128,1024]{1,0:T(8,128)(2,1)} %residual_ref.1, bf16[128,256]{1,0:T(8,128)(2,1)} %query_ref.1, bf16[128,256]{1,0:T(8,128)(2,1)} %forget_ref.1, bf16[128,256]{1,0:T(8,128)(2,1)} %value_ref.1, bf16[128,256]{1,0:T(8,128)(2,1)} %gate_ref.1, f32[1,256]{1,0:T(1,128)} %bitcast.4, f32[1,64]{1,0:T(1,128)} %bitcast.5, ...), custom_call_target="tpu_custom_call" | custom-call | tf_op jit(solution)/shard_map/layer/pallas_call | solution.py:560
  111.6 1.7 %copy.16 = bf16[128,1024]{1,0:T(8,128)(2,1)} copy(bf16[128,1024]{1,0:T(8,128)(2,1)} %layer.1) | data formatting | bytes 524288

commit v4 on v3

--- a/solution.py
+++ b/solution.py
@@ -72,11 +72,14 @@
     tail_s,
     tail_r,
     hid,
-    acc,
     xs,
     xr,
     zs,
     zr,
+    zbs,
+    zbr,
+    xbs,
+    xbr,
     ssem,
     up_r,
     dn_r,
@@ -87,6 +90,7 @@
     nb_r,
     xr_r,
     zr_r,
+    zb_r,
     misc_r,
 ):
     s = lax.axis_index("sp")
@@ -161,6 +165,12 @@
             source = dst
         send(source, dst, sem, at(z, iy))
         send(source, dst, sem, at(z, ic))
+
+    def send_half(part, first):
+        dst, sem = up_slot(z, i)
+        part_rows = pl.ds(part * (depth // 2), depth // 2)
+        src = up_in.at[z3, part_rows]
+        return send(src, dst.at[part_rows], sem, at(z3, i), first)
 
     def prepare_yc(slot, zz):
         dst, sem = slot(zz, i)
@@ -231,8 +241,8 @@
         send(st.at[i], st.at[i], st_r.at[i], at(z, ii))
     far = send_z(up_in, up_slot, z2, z == 3)
     near = send_z(up_in, up_slot, z1, z % 2 == 1)
-    near_dn = send_z(dn_in, dn_slot, z1, z % 2 == 0)
-    last_dn = send_z(dn_in, dn_slot, z3, z == 1)
+    cross = send_half(0, z == 0)
+    near_dn = send_z(dn_in, dn_slot, z1, z == 0)
 
     up[s] = up_in[z]
     dn[s, 0:chunk] = dn_in[z]
@@ -269,6 +279,7 @@
         )
     for k in (3, 2, 1):
         pl.when(z + k < OUTER)(totals[k - 1].start)
+    pl.when(z == 2)(near_dn.start)
     pl.when(z == 2)(near.start)
     forward_yc(up_slot, z, up_in.at[z])
     forward_yc(dn_slot, z, dn_in.at[z])
@@ -365,7 +376,9 @@
 
     share(z, [at(z2, i), at(z1, i), at(z, i, ox)])
     pl.when(z == 0)(near.start)
-    cross = send_z(up_in, up_slot, z3, z > 0)
+    pl.when(z > 0)(cross.start)
+    cross_rest = send_half(1, z > 0)
+    last_dn = send_z(dn_in, dn_slot, z3, False)
     pl.when(z % 2 == 1)(near_dn.start)
     forward_c(up_slot, z)
     forward_c(dn_slot, z)
@@ -388,15 +401,17 @@
     forward_c(up_slot, z2)
     arrived(*nb_slot(z3, x))
     share(z3, [at(z, i, ox)])
-    pl.when(z == 0)(cross.start)
+    pl.when(z == 0)(cross_rest.start)
+    far_dn = send_z(dn_in, dn_slot, z2, z == 3)
+    pl.when(z == 3)(last_dn.start)
     forward_c(up_slot, z1)
     forward_yc(up_slot, z3)
-    send_z(dn_in, dn_slot, z2)
+    pl.when(z < 3)(far_dn.start)
     pl.when(z % 2 == 0)(early_dn)
     later_dn = prepare_yc(dn_slot, z2)
-    pl.when(z % 3 == 0)(later_dn)
+    pl.when(z == 0)(later_dn)
     forward_c(up_slot, z3)
-    pl.when(z != 1)(last_dn.start)
+    pl.when(z < 3)(last_dn.start)
 
     for zz in range(OUTER):
         arrived(*up_slot(zz, ic))
@@ -440,7 +455,7 @@
     send(tail_s, tail_r, misc_r.at[2], {"sp": after, "tp": x})
 
     forward_c(dn_slot, z1)
-    pl.when(z % 3 != 0)(later_dn)
+    pl.when(z > 0)(later_dn)
     forward_yc(dn_slot, z3)
 
     arrived(tail_r, misc_r.at[2])
@@ -473,57 +488,75 @@
         arrived(*dn_slot(zz, ic))
         arrived(*dn_slot(zz, idg))
 
-    def columns(zz, base, store, part):
-        each = deep // 4
-        for j in range(part * each, (part + 1) * each):
-            weight = jnp.concatenate(
-                [dn[base + 2 * j], dn[base + 2 * j + 1]], axis=1
-            )
-            product = jnp.dot(hid[zz], weight, preferred_element_type=f32)
-            store[zz, :, j * step : (j + 1) * step] = product.astype(store.dtype)
-
-    sides = [slice(0, half // 2), slice(half // 2, half)]
-
-    def send_part(src, dst, sem, slot, part, device):
-        side = sides[part]
-        send(src.at[slot, :, side], dst.at[slot, :, side], sem.at[slot, part], device)
-
+    tiles = half // step
+    keep = tiles - 1
     phase = len(pending)
-    order = [(z3, 0), (z2, 0), (z3, 1), (z2, 1), (z1, 0), (z1, 1), (z, 0), (z, 1)]
-    for zz, part in order:
-        columns(zz, ox * deep, xs, part)
-        send_part(xs, xr, xr_r, zz, part, at(z, i, ox))
-
+
+    def tile(j):
+        return slice(j * step, (j + 1) * step)
+
+    def product(zz, base, j):
+        weight = jnp.concatenate([dn[base + 2 * j], dn[base + 2 * j + 1]], axis=1)
+        return jnp.dot(hid[zz], weight, preferred_element_type=f32)
+
+    def both(zz):
+        sides = [product(zz, side * deep, keep) for side in (x, ox)]
+        return jnp.concatenate(sides, axis=1)
+
+    def send_both(slot, value, device):
+        zbs[slot] = value.astype(bf16)
+        send(zbs.at[slot], zbr.at[slot], zb_r.at[slot], device)
+
+    def got_both(slot):
+        arrived(zbr.at[slot], zb_r.at[slot])
+        return zbr[slot].astype(f32)
+
+    def send_tile(src, dst, sem, slot, j, device):
+        lanes = tile(j)
+        send(src.at[slot, :, lanes], dst.at[slot, :, lanes], sem.at[slot, j], device)
+
+    send_both(0, both(z3), at(z1, i))
+    send_both(1, both(z1), at(z1, i))
+    order = [(zz, j) for j in range(keep) for zz in (z3, z2)]
+    order += [(zz, j) for zz in (z1, z) for j in range(keep)]
+    for zz, j in order:
+        xs[zz, :, tile(j)] = product(zz, ox * deep, j).astype(bf16)
+        send_tile(xs, xr, xr_r, zz, j, at(z, i, ox))
     for copy in pending[:phase]:
         copy.wait_send()
 
-    def summed(zz, part):
-        side = sides[part]
-        columns(zz, x * deep, acc, part)
-        arrived(xr.at[zz, :, side], xr_r.at[zz, part])
-        return acc[zz, :, side] + xr[zz, :, side].astype(f32)
-
-    def received(slot, part):
-        side = sides[part]
-        arrived(zr.at[slot, :, side], zr_r.at[slot, part])
-        return zr[slot, :, side].astype(f32)
-
-    def pass_on(slot, part, value, device):
-        zs[slot, :, sides[part]] = value.astype(bf16)
-        send_part(zs, zr, zr_r, slot, part, device)
+    def summed(zz, j):
+        value = product(zz, x * deep, j)
+        arrived(xr.at[zz, :, tile(j)], xr_r.at[zz, j])
+        return value + xr[zz, :, tile(j)].astype(f32)
+
+    def received(slot, j):
+        arrived(zr.at[slot, :, tile(j)], zr_r.at[slot, j])
+        return zr[slot, :, tile(j)].astype(f32)
+
+    def pass_on(slot, j, value, device):
+        zs[slot, :, tile(j)] = value.astype(bf16)
+        send_tile(zs, zr, zr_r, slot, j, device)
 
     pass_on(0, 0, summed(z3, 0), at(z1, i))
-    value = summed(z2, 0)
-    pass_on(2, 0, value + received(0, 0), at(z2, i))
-    pass_on(0, 1, summed(z3, 1), at(z1, i))
-    value = summed(z2, 1)
-    pass_on(2, 1, value + received(0, 1), at(z2, i))
-    for part in range(2):
-        pass_on(1, part, summed(z1, part), at(z1, i))
-    for part in range(2):
-        side = sides[part]
-        own = summed(z, part) + received(1, part) + received(2, part)
-        out_ref[:, side] = (stream[:, side] + own).astype(bf16)
+    send_both(2, both(z2) + got_both(0), at(z2, i))
+    for j in range(1, keep):
+        pass_on(0, j, summed(z3, j), at(z1, i))
+    for j in range(keep):
+        value = summed(z2, j)
+        pass_on(2, j, value + received(0, j), at(z2, i))
+    for j in range(keep):
+        pass_on(1, j, summed(z1, j), at(z1, i))
+    pair = both(z) + got_both(1)
+    pair = pair + got_both(2)
+    xbs[...] = pair[:, step:].astype(bf16)
+    send(xbs, xbr, zb_r.at[3], at(z, i, ox))
+    for j in range(keep):
+        own = summed(z, j) + received(1, j) + received(2, j)
+        out_ref[:, tile(j)] = (stream[:, tile(j)] + own).astype(bf16)
+    arrived(xbr, zb_r.at[3])
+    own = pair[:, :step] + xbr[...].astype(f32)
+    out_ref[:, tile(keep)] = (stream[:, tile(keep)] + own).astype(bf16)
 
     for copy in pending[phase:]:
         copy.wait_send()
@@ -580,12 +613,15 @@
             pltpu.VMEM((2 * OUTER, span), f32),
             pltpu.VMEM((2 * OUTER, span), f32),
             pltpu.VMEM((OUTER, rows, padded), bf16),
-            pltpu.VMEM((OUTER, rows, my_width), f32),
             pltpu.VMEM((OUTER, rows, my_width), bf16),
             pltpu.VMEM((OUTER, rows, my_width), bf16),
             pltpu.VMEM((3, rows, my_width), bf16),
             pltpu.VMEM((3, rows, my_width), bf16),
-            dma((80,)),
+            pltpu.VMEM((3, rows, 4 * LANES), bf16),
+            pltpu.VMEM((3, rows, 4 * LANES), bf16),
+            pltpu.VMEM((rows, 2 * LANES), bf16),
+            pltpu.VMEM((rows, 2 * LANES), bf16),
+            dma((96,)),
             dma((blocks,)),
             dma((blocks,)),
             dma((INNER,)),
@@ -593,8 +629,9 @@
             dma((OUTER,)),
             pltpu.SemaphoreType.REGULAR,
             dma((2 * OUTER,)),
-            dma((OUTER, 2)),
-            dma((3, 2)),
+            dma((OUTER, 4)),
+            dma((3, 4)),
+            dma((4,)),
             dma((3,)),
         ],
         compiler_params=pltpu.CompilerParams(

time: 114 us -> 109 us (0.956)
  Pallas kernels: 112 us -> 107 us
    pallas_call x1, Pallas kernels: 112 us -> 107 us  [fused_layer(): pl.pallas_call(functools.partial(layer_kernel, full, extra), out_shape=ja...]
where the time goes in v4:
time: 109 us; the launch traced here: 108 us
  Pallas kernels  107 us (98%)
  local copies, waits for them, and re-layouts  1.67 us (2%)
    pallas_call x1, Pallas kernels, fused_layer(): pl.pallas_call(functools.partial(layer_kernel, full, extra), out_shape=ja...  107 us

profile of v4, /device:TPU:0, one launch (start us, length us, event | category | flops | bytes accessed | tf_op | source)
XLA Modules:
  0.0 108.4 jit_solution(16934156132589387623)
XLA Ops:
  0.0 106.7 %layer.1 = bf16[128,1024]{1,0:T(8,128)(2,1)} custom-call(bf16[128,1024]{1,0:T(8,128)(2,1)} %residual_ref.1, bf16[128,256]{1,0:T(8,128)(2,1)} %query_ref.1, bf16[128,256]{1,0:T(8,128)(2,1)} %forget_ref.1, bf16[128,256]{1,0:T(8,128)(2,1)} %value_ref.1, bf16[128,256]{1,0:T(8,128)(2,1)} %gate_ref.1, f32[1,256]{1,0:T(1,128)} %bitcast.4, f32[1,64]{1,0:T(1,128)} %bitcast.5, ...), custom_call_target="tpu_custom_call" | custom-call | tf_op jit(solution)/shard_map/layer/pallas_call | solution.py:593
  106.7 1.7 %copy.16 = bf16[128,1024]{1,0:T(8,128)(2,1)} copy(bf16[128,1024]{1,0:T(8,128)(2,1)} %layer.1) | data formatting | bytes 524288

commit v5 on v4

--- a/solution.py
+++ b/solution.py
@@ -409,9 +409,9 @@
     pl.when(z < 3)(far_dn.start)
     pl.when(z % 2 == 0)(early_dn)
     later_dn = prepare_yc(dn_slot, z2)
-    pl.when(z == 0)(later_dn)
     forward_c(up_slot, z3)
     pl.when(z < 3)(last_dn.start)
+    pl.when(z % 3 == 0)(later_dn)
 
     for zz in range(OUTER):
         arrived(*up_slot(zz, ic))
@@ -455,7 +455,7 @@
     send(tail_s, tail_r, misc_r.at[2], {"sp": after, "tp": x})
 
     forward_c(dn_slot, z1)
-    pl.when(z > 0)(later_dn)
+    pl.when(z % 3 != 0)(later_dn)
     forward_yc(dn_slot, z3)
 
     arrived(tail_r, misc_r.at[2])
@@ -592,7 +592,7 @@
     span = 2 * chunk
     return pl.pallas_call(
         functools.partial(layer_kernel, full, extra),
-        out_shape=jax.ShapeDtypeStruct((rows, my_width), bf16),
+        out_shape=pltpu.VMEM((rows, my_width), bf16),
         in_specs=[vmem] * 14,
         out_specs=vmem,
         scratch_shapes=[

time: 109 us -> 106 us (0.972)
  Pallas kernels: 107 us -> 105 us
    pallas_call x1, Pallas kernels: 107 us -> 105 us  [fused_layer(): pl.pallas_call(functools.partial(layer_kernel, full, extra), out_shape=pl...]
where the time goes in v5:
time: 106 us
  Pallas kernels  105 us (99%)
    pallas_call x1, Pallas kernels, fused_layer(): pl.pallas_call(functools.partial(layer_kernel, full, extra), out_shape=pl...  105 us

profile of v5, /device:TPU:0, one launch (start us, length us, event | category | flops | bytes accessed | tf_op | source)
XLA Modules:
  0.0 105.7 jit_solution(14873250909861208134)
XLA Ops:
  0.0 105.0 %layer.1 = bf16[128,1024]{1,0:T(8,128)(2,1)S(1)} custom-call(bf16[128,1024]{1,0:T(8,128)(2,1)} %residual_ref.1, bf16[128,256]{1,0:T(8,128)(2,1)} %query_ref.1, bf16[128,256]{1,0:T(8,128)(2,1)} %forget_ref.1, bf16[128,256]{1,0:T(8,128)(2,1)} %value_ref.1, bf16[128,256]{1,0:T(8,128)(2,1)} %gate_ref.1, f32[1,256]{1,0:T(1,128)} %bitcast.4, f32[1,64]{1,0:T(1,128)} %bitcast.5, ...), custom_call_target="tpu_custom_call" | custom-call | tf_op jit(solution)/shard_map/layer/pallas_call | solution.py:593
  105.0 0.7 copy.16

commit v6 on v5

--- a/solution.py
+++ b/solution.py
@@ -539,9 +539,9 @@
         send_tile(zs, zr, zr_r, slot, j, device)
 
     pass_on(0, 0, summed(z3, 0), at(z1, i))
-    send_both(2, both(z2) + got_both(0), at(z2, i))
     for j in range(1, keep):
         pass_on(0, j, summed(z3, j), at(z1, i))
+    send_both(2, both(z2) + got_both(0), at(z2, i))
     for j in range(keep):
         value = summed(z2, j)
         pass_on(2, j, value + received(0, j), at(z2, i))

time: 106 us -> 110 us (1.038)
  Pallas kernels: 105 us -> 109 us
    pallas_call x1, Pallas kernels: 105 us -> 109 us  [fused_layer(): pl.pallas_call(functools.partial(layer_kernel, full, extra), out_shape=pl...]
where the time goes in v6:
time: 110 us
  Pallas kernels  109 us (99%)
    pallas_call x1, Pallas kernels, fused_layer(): pl.pallas_call(functools.partial(layer_kernel, full, extra), out_shape=pl...  109 us

profile of v6, /device:TPU:0, one launch (start us, length us, event | category | flops | bytes accessed | tf_op | source)
XLA Modules:
  0.0 110.1 jit_solution(15081548339454881716)
XLA Ops:
  0.0 109.4 %layer.1 = bf16[128,1024]{1,0:T(8,128)(2,1)S(1)} custom-call(bf16[128,1024]{1,0:T(8,128)(2,1)} %residual_ref.1, bf16[128,256]{1,0:T(8,128)(2,1)} %query_ref.1, bf16[128,256]{1,0:T(8,128)(2,1)} %forget_ref.1, bf16[128,256]{1,0:T(8,128)(2,1)} %value_ref.1, bf16[128,256]{1,0:T(8,128)(2,1)} %gate_ref.1, f32[1,256]{1,0:T(1,128)} %bitcast.4, f32[1,64]{1,0:T(1,128)} %bitcast.5, ...), custom_call_target="tpu_custom_call" | custom-call | tf_op jit(solution)/shard_map/layer/pallas_call | solution.py:593
  109.4 0.7 copy.16
